TPU v7x, 256 devices: a 2x2x32 block of a 4x8x32 slice. The times are simulated.
256 devices in a mesh: grp: 4 (over y, x), ep: 64 (over z, core).
Axes of the slice: x: 2, y: 2, z: 32, core: 2. Of those that a mesh axis runs over, the one named last changes fastest.
The devices are a block of a 4x8x32 slice.
Arguments:
- tokens: bfloat16 [32768, 2048], P(('grp', 'ep')), parts along dimension 0, may hold values from -6 to 6
- norm_gain: float32 [2048], replicated, may hold values from 0.1 to 1.9
- expert_ids: int32 [32768, 2], P(('grp', 'ep')), parts along dimension 0, may hold values from 0 to 15, all different within a row; in each aligned block of 128 rows (0 to 127, 128 to 255, ...) at most 32 rows name the same one
- route_weight: float32 [32768, 2], P(('grp', 'ep')), parts along dimension 0, may hold values from 0.1 to 1
- gate_weight: bfloat16 [64, 2048, 512], P('ep'), may hold values from -0.375 to 0.375
- up_weight: bfloat16 [64, 2048, 512], P('ep'), may hold values from -0.375 to 0.375
- down_weight: bfloat16 [64, 512, 2048], P('ep'), may hold values from -0.03125 to 0.03125
Outputs:
- combined: bfloat16 [32768, 2048], P(('grp', 'ep')), parts along dimension 0
There are 4 independent parts, one for each index of `grp`. A program takes and returns all parts, laid end to end along the dimension named above; an argument that names none is the same for every part. Nothing has to cross between parts.
Inputs may be any that keep to these rules, and one draw needn't show every extreme that they name: `expert_ids`: each token names 2 different experts; among the tokens of one device no expert is named more than 32 times, and in every draw some expert is named exactly 32 times by the tokens of some device.
All inputs are finite; a program needn't handle non-finite values.
Results may differ from a plain program's by a relative error of at most 0.0078.
Values may be sent and summed in bfloat16 or wider, within the bound.
No kernel may reach another device: no remote copies, remote signals or barrier semaphores. Data moves between devices by JAX's collectives and lax.ppermute only.
A program may use at most 128 MiB of HBM per device.

v0:
```python
import jax
import jax.numpy as jnp
from jax import lax
from jax.sharding import PartitionSpec as P

SPLIT = 4


EPSILON = 1e-05
clamp_limit = 7.0
sigmoid_slope = 1.702


def swapped(array, axis, bit):
    return lax.ppermute(array, axis, [(i, i ^ 1 << bit) for i in range(lax.axis_size(axis))])


def layer_norm(tokens, norm_gain):
    values = tokens.astype(jnp.float32)
    center = values - jnp.mean(values, axis=-1, keepdims=True)
    spread = jnp.mean(center * center, axis=-1, keepdims=True)
    return (center * lax.rsqrt(spread + EPSILON) * norm_gain).astype(jnp.bfloat16)


def expert_rows(block_rows, gate_weight, up_weight, down_weight):
    gate_pre = jnp.einsum(
        "scd,df->scf", block_rows, gate_weight[0], preferred_element_type=jnp.float32
    )
    up_pre = jnp.einsum("scd,df->scf", block_rows, up_weight[0], preferred_element_type=jnp.float32)
    gate_cut = jnp.minimum(gate_pre, clamp_limit)
    up_cut = jnp.clip(up_pre, -clamp_limit, clamp_limit)
    active = ((up_cut + 1.0) * (gate_cut * jax.nn.sigmoid(gate_cut * sigmoid_slope))).astype(
        jnp.bfloat16
    )
    return jnp.einsum("scf,fd->scd", active, down_weight[0], preferred_element_type=jnp.float32)


def body(tokens, norm_gain, expert_ids, route_weight, gate_weight, up_weight, down_weight):
    normed = layer_norm(tokens, norm_gain)
    devices = lax.axis_size("ep")
    experts = devices // SPLIT
    tok_rows = tokens.shape[0]
    top_count = expert_ids.shape[1]
    width = tokens.shape[1]
    capacity = min(tok_rows, 2 * tok_rows * top_count // experts)
    quarter = capacity // SPLIT
    levels = SPLIT.bit_length() - 1
    position = lax.axis_index("ep")
    flat_ids = expert_ids.reshape(-1)
    onehot = (flat_ids[:, None] == jnp.arange(experts, dtype=jnp.int32)[None, :]).astype(jnp.int32)
    earlier = jnp.cumsum(onehot, axis=0) - onehot
    slot_index = jnp.sum(earlier * onehot, axis=1)
    target = flat_ids * capacity + slot_index
    owners = jnp.arange(flat_ids.shape[0], dtype=jnp.int32) // top_count
    slot_token = jnp.full((experts * capacity,), tok_rows, jnp.int32).at[target].set(owners)
    padded = jnp.concatenate([normed, jnp.zeros((1, width), jnp.bfloat16)], axis=0)
    outgoing = jnp.take(padded, slot_token, axis=0).reshape(experts, capacity, width)
    pieces = outgoing.reshape(devices, quarter, width)
    gathered = lax.all_to_all(pieces, "ep", split_axis=0, concat_axis=0, tiled=True)
    for bit_level in range(levels):
        partner = swapped(gathered, "ep", bit_level)
        upper_bit = position >> bit_level & 1
        first_half = jnp.where(upper_bit == 1, partner, gathered)
        second_half = jnp.where(upper_bit == 1, gathered, partner)
        gathered = jnp.concatenate([first_half, second_half], axis=1)
    partial_value = expert_rows(gathered, gate_weight, up_weight, down_weight)
    length = capacity
    for bit_level in reversed(range(levels)):
        length = length // 2
        upper_bit = position >> bit_level & 1
        kept_rows = lax.dynamic_slice_in_dim(partial_value, upper_bit * length, length, 1)
        sent_rows = lax.dynamic_slice_in_dim(partial_value, (1 - upper_bit) * length, length, 1)
        partial_value = kept_rows + swapped(sent_rows.astype(jnp.bfloat16), "ep", bit_level).astype(
            sent_rows.dtype
        )
    finished = partial_value.astype(jnp.bfloat16)
    returned = lax.all_to_all(finished, "ep", split_axis=0, concat_axis=0, tiled=True)
    results = returned.reshape(experts * capacity, width)
    picked = jnp.take(results, target, axis=0).reshape(tok_rows, top_count, width)
    combined = jnp.sum(route_weight[:, :, None] * picked.astype(jnp.float32), axis=1)
    return combined.astype(jnp.bfloat16)


def solution(mesh):
    placed = (
        P(("grp", "ep"), None),
        P(),
        P(("grp", "ep"), None),
        P(("grp", "ep"), None),
        P("ep", None, None),
        P("ep", None, None),
        P("ep", None, None),
    )
    return jax.shard_map(
        body, mesh=mesh, in_specs=placed, out_specs=P(("grp", "ep"), None), check_vma=False
    )
```

profile of v0, /device:TPU:46, one launch (start us, length us, event | category | flops | bytes accessed | tf_op | source)
XLA Modules:
  0.0 716.8 jit_solution(9506049461779293233)
XLA Ops:
  0.0 0.9 copy.16
  1.2 0.7 broadcast_multiply_fusion
  1.9 0.6 reduce-window.6
  3.1 1.4 scatter_custom_fusion
  4.5 1.2 convert_reduce_fusion
  5.7 1.3 fusion.13
  7.2 1.4 fusion.15
  8.7 3.3 gather_fusion
  12.0 1.8 bitcast_select_fusion
  13.8 233.2 %all_to_all.10 = bf16[64,8,2048]{2,1,0:T(8,128)(2,1)} all-to-all(bf16[64,8,2048]{2,1,0:T(8,128)(2,1)S(1)} %bitcast_select_fusion), channel_id=1, replica_groups=mesh['grp'=4,'ep'=64] {'ep'}, dimensions={0} | all-to-all | bytes 4194304 | tf_op jit(solution)/shard_map/all_to_all | solution.py:59
  247.0 4.5 collective-permute-done
  251.5 2.5 broadcast_select_fusion.3
  254.0 2.5 pad_maximum_fusion.3
  256.6 0.7 copy-done.4
  257.3 92.9 %collective-permute-done.1 = bf16[64,16,2048]{2,1,0:T(8,128)(2,1)} collective-permute-done((bf16[64,16,2048]{2,1,0:T(8,128)(2,1)}, bf16[64,16,2048]{2,1,0:T(8,128)(2,1)}, u32[]{:S(2)}, u32[]{:S(2)}) %collective-permute-start.1) | collective-permute-done | bytes 4194336 | tf_op jit(solution)/shard_map/ppermute | solution.py:15
  350.3 5.0 broadcast_select_fusion.1
  355.3 2.0 copy-done.5
  357.2 1.3 copy-done.6
  358.5 6.0 fusion.1
  364.6 16.5 %fusion.2 = f32[64,32,2048]{2,1,0:T(8,128)} fusion(f32[64,32,512]{2,1,0:T(8,128)} %fusion.1, bf16[64,16,2048]{2,1,0:T(8,128)(2,1)} %copy-done.6, bf16[64,16,2048]{2,1,0:T(8,128)(2,1)} %copy-done.5, bf16[1,512,2048]{2,1,0:T(8,128)(2,1)S(1)} %copy-done, bf16[1,2048,512]{2,1,0:T(8,128)(2,1)} %param.11), kind=kOutput, calls=%fused_computation.14 | convolution fusion | flops 8617197568 | bytes 33554432 | tf_op jit(solution)/shard_map/scf,fd->scd/dot_general | solution.py:35
  381.1 6.0 dynamic-slice_convert_fusion
  387.4 91.8 %collective-permute-done.2 = bf16[64,16,2048]{2,1,0:T(8,128)(2,1)} collective-permute-done((bf16[64,16,2048]{2,1,0:T(8,128)(2,1)}, bf16[64,16,2048]{2,1,0:T(8,128)(2,1)}, u32[]{:S(2)}, u32[]{:S(2)}) %collective-permute-start.2) | collective-permute-done | bytes 4194336 | tf_op jit(solution)/shard_map/ppermute | solution.py:15
  479.1 5.9 convert_add_fusion
  485.1 3.2 copy-done.2
  488.3 0.3 dynamic-slice_convert_fusion.1
  488.8 4.3 collective-permute-done.3
  493.0 4.9 add_convert_fusion
  498.0 7.5 %all-to-all-start.1 = ((bf16[64,8,2048]{2,1,0:T(8,128)(2,1)}), bf16[64,8,2048]{2,1,0:T(8,128)(2,1)}, u32[]{:S(2)}, u32[]{:S(2)}) async-start(bf16[64,8,2048]{2,1,0:T(8,128)(2,1)} %add_convert_fusion), calls=%async_computation.1 | async-start | bytes 4194304 | tf_op jit(solution)/shard_map/all_to_all | solution.py:77
  506.0 198.6 %all-to-all-done.1 = bf16[64,8,2048]{2,1,0:T(8,128)(2,1)} async-done(((bf16[64,8,2048]{2,1,0:T(8,128)(2,1)}), bf16[64,8,2048]{2,1,0:T(8,128)(2,1)}, u32[]{:S(2)}, u32[]{:S(2)}) %all-to-all-start.1) | async-done | bytes 2097184 | tf_op jit(solution)/shard_map/all_to_all | solution.py:77
  704.7 4.4 gather_fusion.1
  709.0 1.5 gather.15
  710.6 6.2 multiply_reduce_fusion
  (44 shorter events, 2.1 us)
Async XLA Ops:
  0.0 364.6 %copy-start = (bf16[1,512,2048]{2,1,0:T(8,128)(2,1)S(1)}, bf16[1,512,2048]{2,1,0:T(8,128)(2,1)}, u32[]{:S(2)}) copy-start(bf16[1,512,2048]{2,1,0:T(8,128)(2,1)} %param.13) | copy-start | bytes 6291460
  247.0 4.5 collective-permute-start
  254.0 2.6 copy-start.3
  254.0 3.3 copy-start.4
  257.3 92.9 %collective-permute-start.1 = (bf16[64,16,2048]{2,1,0:T(8,128)(2,1)}, bf16[64,16,2048]{2,1,0:T(8,128)(2,1)}, u32[]{:S(2)}, u32[]{:S(2)}) collective-permute-start(bf16[64,16,2048]{2,1,0:T(8,128)(2,1)} %pad_maximum_fusion.3), channel_id=1, source_target_pairs={{0,2},{1,3},{2,0},{3,1},{4,6},{5,7},{6,4},{7,5},{8,10},{9,11},{10,... | collective-permute-start | bytes 12582920 | tf_op jit(solution)/shard_map/ppermute | solution.py:15
  257.3 101.2 %copy-start.9 = (bf16[1,2048,512]{2,1,0:T(8,128)(2,1)S(1)}, bf16[1,2048,512]{2,1,0:T(8,128)(2,1)}, u32[]{:S(2)}) copy-start(bf16[1,2048,512]{2,1,0:T(8,128)(2,1)} %param.12) | copy-start | bytes 6291460
  355.3 2.0 copy-start.5
  355.3 3.2 copy-start.6
  387.1 92.1 %collective-permute-start.2 = (bf16[64,16,2048]{2,1,0:T(8,128)(2,1)}, bf16[64,16,2048]{2,1,0:T(8,128)(2,1)}, u32[]{:S(2)}, u32[]{:S(2)}) collective-permute-start(bf16[64,16,2048]{2,1,0:T(8,128)(2,1)} %dynamic-slice_convert_fusion), channel_id=1, source_target_pairs={{0,2},{1,3},{2,0},{3,1},{4,6},{5,7},{6,4},{7,5},{8,10},{9,11},{10,... | collective-permute-start | bytes 12582920 | tf_op jit(solution)/shard_map/ppermute | solution.py:15
  485.1 3.2 copy-start.2
  488.6 4.4 collective-permute-start.3
  498.0 7.8 %copy-start.7 = (s32[128,2]{0,1:T(2,128)S(1)}, s32[128,2]{0,1:T(2,128)}, u32[]{:S(2)}) copy-start(s32[128,2]{0,1:T(2,128)} %param.9) | copy-start | bytes 3076
  498.0 7.9 %copy-start.8 = (f32[128,2]{0,1:T(2,128)S(1)}, f32[128,2]{0,1:T(2,128)}, u32[]{:S(2)}) copy-start(f32[128,2]{0,1:T(2,128)} %param.10) | copy-start | bytes 3076
  498.0 206.7 %all-to-all-start.1 = ((bf16[64,8,2048]{2,1,0:T(8,128)(2,1)}), bf16[64,8,2048]{2,1,0:T(8,128)(2,1)}, u32[]{:S(2)}, u32[]{:S(2)}) async-start(bf16[64,8,2048]{2,1,0:T(8,128)(2,1)} %add_convert_fusion), calls=%async_computation.1 | async-start | bytes 4194304 | tf_op jit(solution)/shard_map/all_to_all | solution.py:77
  704.7 12.1 %copy-start.1 = (bf16[1,512,2048]{2,1,0:T(8,128)(2,1)S(1)}, bf16[1,512,2048]{2,1,0:T(8,128)(2,1)}, u32[]{:S(2)}) copy-start(bf16[1,512,2048]{2,1,0:T(8,128)(2,1)} %param.13) | copy-start | bytes 6291460
where the time goes:
time: 717 us
  waiting for transfers between devices  392 us (55%)
  blocking collectives  233 us (32%)
  other arithmetic  34.3 us (5%)
  local copies, waits for them, and re-layouts  26.5 us (4%)
  matrix products  22.5 us (3%)
  starting transfers between devices  7.96 us (1%)
    all_to_all x1, blocking collectives, body(): lax.all_to_all(pieces, 'ep', split_axis=0, concat_axis=0, tiled=True)  233 us
    all_to_all x1, waiting for transfers between devices, body(): lax.all_to_all(finished, 'ep', split_axis=0, concat_axis=0, tiled=True)  199 us
    ppermute x4, waiting for transfers between devices, swapped(): lax.ppermute(array, axis, [(i, i ^ 1 << bit) for i in range(lax.axis_size...  193 us
    dot_general x1, matrix products, expert_rows(): jnp.einsum('scf,fd->scd', active, down_weight[0], preferred_element_type=...  16.5 us
  transfers between devices with their start and end apart: 5, of which 5 were waited for; matrix products, arithmetic and copies ran while one was open for 0% of the time, Pallas kernels for 0%

commit v1 on v0

v1 whole, which is shorter than its diff:
```python
from functools import partial

import jax
import jax.numpy as jnp
from jax import lax
from jax.experimental import pallas as pl
from jax.experimental.pallas import tpu as pltpu
from jax.sharding import PartitionSpec as P

INTERPRET = False
LANES = 128
SUB = 32
META = 16
EPSILON = 1e-05
clamp_limit = 7.0
sigmoid_slope = 1.702
f32 = jnp.float32
bf16 = jnp.bfloat16


def shifted(array, step):
    size = lax.axis_size("ep")
    return lax.ppermute(array, "ep", [(i, (i + step) % size) for i in range(size)])


def iota(shape, axis):
    return lax.broadcasted_iota(jnp.int32, shape, axis)


def reaches(ids, pair, parity, experts):
    half = experts // 2
    ahead = ids - pair
    ahead = jnp.where(ahead < 0, ahead + experts, ahead)
    behind = experts - ahead
    up_even = jnp.where(ahead < half, 2 * ahead + 1, 0)
    up_odd = jnp.where((ahead >= 1) & (ahead <= half), 2 * ahead, 0)
    down_even = jnp.where(ahead >= half, 2 * behind, 0)
    down_odd = jnp.where(ahead == 0, 1, jnp.where(ahead > half, 2 * behind + 1, 0))
    even = parity == 0
    return jnp.where(even, up_even, up_odd), jnp.where(even, down_even, down_odd)


def prepare_kernel(where_ref, tokens_ref, gain_ref, ids_ref, weight_ref,
                   upa_ref, upb_ref, downa_ref, downb_ref, upt_ref, downt_ref, *, experts):
    rows, width = tokens_ref.shape
    pair, parity = where_ref[0], where_ref[1]
    values = tokens_ref[...].astype(f32)
    center = values - jnp.mean(values, axis=-1, keepdims=True)
    spread = jnp.mean(center * center, axis=-1, keepdims=True)
    normed = (center * lax.rsqrt(spread + EPSILON) * gain_ref[...]).astype(bf16)

    ids = ids_ref[...].astype(f32)
    weights = weight_ref[...]
    high = weights.astype(bf16).astype(f32)
    middle = (weights - high).astype(bf16).astype(f32)
    low = weights - high - middle
    lane = iota((rows, LANES), 1)
    table = jnp.zeros((rows, LANES), f32)
    columns = [ids[:, 0:1], ids[:, 1:2]]
    for k in range(2):
        columns += [high[:, k:k + 1], middle[:, k:k + 1], low[:, k:k + 1]]
    for number, column in enumerate(columns):
        table = jnp.where(lane == number, column, table)
    meta = table.T
    meta_bf = meta[0:META, :].astype(bf16)
    first_c, second_c = ids_ref[:, 0:1], ids_ref[:, 1:2]
    first_r, second_r = meta[0:1, :].astype(jnp.int32), meta[1:2, :].astype(jnp.int32)
    reach_c = [jnp.maximum(a, b) for a, b in zip(
        reaches(first_c, pair, parity, experts), reaches(second_c, pair, parity, experts))]
    reach_r = [jnp.maximum(a, b) for a, b in zip(
        reaches(first_r, pair, parity, experts), reaches(second_r, pair, parity, experts))]
    sub_i, lane_i = iota((rows, rows), 0), iota((rows, rows), 1)
    for way, (a_ref, b_ref, t_ref) in enumerate(
            ((upa_ref, upb_ref, upt_ref), (downa_ref, downb_ref, downt_ref))):
        col, row = reach_c[way], reach_r[way]
        ahead_c = (row > col) | ((row == col) & (lane_i < sub_i))
        ahead_r = (col > row) | ((col == row) & (sub_i < lane_i))
        rank_c = jnp.sum(ahead_c.astype(f32), axis=1, keepdims=True).astype(jnp.int32)
        rank_r = jnp.sum(ahead_r.astype(f32), axis=0, keepdims=True).astype(jnp.int32)
        back = (rank_c == lane_i).astype(f32).astype(bf16)
        order = (rank_r == sub_i).astype(f32).astype(bf16)
        t_ref[...] = back
        ordered = jnp.dot(order, normed, preferred_element_type=f32).astype(bf16)
        a_ref[pl.ds(SUB * (width // LANES), META), :] = jnp.dot(
            meta_bf, back, preferred_element_type=f32).astype(bf16)
        for sub in range(4):
            put_sub(a_ref, b_ref, sub, ordered[SUB * sub:SUB * (sub + 1)], META)


def sub_place(sub, blocks, gap):
    return {0: (0, 0), 1: (1, 0), 2: (1, SUB * blocks), 3: (0, SUB * blocks + gap)}[sub]


def put_sub(a_ref, b_ref, sub, rows, gap):
    blocks = rows.shape[1] // LANES
    which, start = sub_place(sub, blocks, gap)
    ref = (a_ref, b_ref)[which]
    for c in range(blocks):
        ref[start + SUB * c:start + SUB * (c + 1), :] = rows[:, LANES * c:LANES * (c + 1)]


def get_block(refs, subs, blocks, gap, c, axis=0):
    parts = []
    for sub in range(subs):
        which, start = sub_place(sub, blocks, gap)
        parts.append(refs[which][start + SUB * c:start + SUB * (c + 1), :])
    return parts[0] if subs == 1 else jnp.concatenate(parts, axis=0)


def expert_kernel(*refs, specs, steps):
    count = len(specs)
    where_ref = refs[0]
    cursor = 1
    sources = []
    for subs, _ in specs:
        take = 2 if subs > 1 else 1
        sources.append(refs[cursor:cursor + take])
        cursor += take
    gates, ups, downs = refs[cursor:cursor + 2], refs[cursor + 2:cursor + 4], refs[cursor + 4:cursor + 6]
    cursor += 6
    results = []
    for subs, _ in specs:
        take = 2 if subs > 1 else 1
        results.append(refs[cursor:cursor + take])
        cursor += take
    rows_ref, sum_ref, hot_ref, factor_ref = refs[cursor:cursor + 4]
    width = rows_ref.shape[1]
    blocks = width // LANES
    step = pl.program_id(0)
    expert, parity = where_ref[0], where_ref[1]

    @pl.when(step == 0)
    def _():
        before = (iota((LANES, LANES), 0) < iota((LANES, LANES), 1)).astype(f32).astype(bf16)
        lane = iota((1, LANES), 1)
        for number, (subs, only) in enumerate(specs):
            meta = sources[number][0][SUB * blocks:SUB * blocks + META, :].astype(f32)
            target = expert.astype(f32)
            valid = lane < SUB * subs
            if only is not None:
                valid = valid & (lane < jnp.where(parity == only, LANES, 0))
            first = (meta[0:1] == target) & valid
            second = (meta[1:2] == target) & valid
            factor = jnp.where(first, (meta[2:3] + meta[3:4]) + meta[4:5], 0.0)
            factor = factor + jnp.where(second, (meta[5:6] + meta[6:7]) + meta[7:8], 0.0)
            match = jnp.where(first | second, 1.0, 0.0)
            slot = jnp.dot(jnp.broadcast_to(match, (16, LANES)).astype(bf16), before,
                           preferred_element_type=f32)[0:1]
            slot = jnp.where(match > 0.0, slot, -1.0)
            hot = (slot == iota((SUB, LANES), 0).astype(f32)).astype(f32)
            span = pl.ds(SUB * number, SUB)
            factor_ref[span, :] = jnp.broadcast_to(
                jnp.sum(hot * factor, axis=1, keepdims=True), (SUB, LANES))
            hot_ref[span, :] = hot
            hot = hot[:, :SUB * subs].astype(bf16)
            for c in range(blocks):
                rows_ref[span, LANES * c:LANES * (c + 1)] = jnp.dot(
                    hot, get_block(sources[number], subs, blocks, META, c),
                    preferred_element_type=f32).astype(bf16)

    def partial_sum(gate_ref, up_ref, down_ref):
        rows = rows_ref[...]
        gate = jnp.minimum(jnp.dot(rows, gate_ref[0], preferred_element_type=f32), clamp_limit)
        up = jnp.clip(jnp.dot(rows, up_ref[0], preferred_element_type=f32), -clamp_limit, clamp_limit)
        active = ((up + 1.0) * (gate * jax.nn.sigmoid(gate * sigmoid_slope))).astype(bf16)
        return jnp.dot(active, down_ref[0], preferred_element_type=f32)

    @pl.when(step == 0)
    def _():
        sum_ref[...] = partial_sum(gates[0], ups[0], downs[0])

    @pl.when((step > 0) & (step < steps))
    def _():
        sum_ref[...] += partial_sum(gates[0], ups[0], downs[0])

    @pl.when(step >= steps)
    def _():
        sum_ref[...] += partial_sum(gates[1], ups[1], downs[1])

    @pl.when(step == 2 * steps - 1)
    def _():
        for number, (subs, _) in enumerate(specs):
            span = pl.ds(SUB * number, SUB)
            weighted = (sum_ref[span, :] * factor_ref[span, 0:1]).astype(bf16)
            spread = hot_ref[span, :].T[:SUB * subs].astype(bf16)
            dense = jnp.dot(spread, weighted, preferred_element_type=f32).astype(bf16)
            pair = results[number]
            for sub in range(subs):
                put_sub(pair[0], pair[-1], sub, dense[SUB * sub:SUB * (sub + 1)], 0)


def finish_kernel(*refs):
    *messages, upt_ref, downt_ref, out_ref = refs
    width = out_ref.shape[1]
    blocks = width // LANES
    ways = ((upt_ref, messages[0:2]), (upt_ref, messages[2:4]), (downt_ref, messages[4:6]))
    for c in range(blocks):
        total = None
        for back_ref, pair in ways:
            part = jnp.dot(back_ref[...], get_block(pair, 4, blocks, 0, c), preferred_element_type=f32)
            total = part if total is None else total + part
        out_ref[:, LANES * c:LANES * (c + 1)] = total.astype(bf16)


VMEM = pl.BlockSpec(memory_space=pltpu.VMEM)
SMEM = pl.BlockSpec(memory_space=pltpu.SMEM)


def apply_experts(where, sources, specs, weights, partner_weights):
    width = weights[0].shape[1]
    hidden = weights[0].shape[2]
    tile = min(256, hidden)
    steps = hidden // tile
    blocks = width // LANES
    flat, out_shapes, in_specs, out_specs = [], [], [SMEM], []
    held = lambda shape: pl.BlockSpec(shape, lambda i: (0, 0), pipeline_mode=pl.Buffered(1))
    for (subs, _), pair in zip(specs, sources):
        flat += list(pair)
        in_specs += [held(x.shape) for x in pair]
        sizes = message_rows(subs, blocks)
        out_shapes += [jax.ShapeDtypeStruct((n, LANES), bf16) for n in sizes]
        out_specs += [held((n, LANES)) for n in sizes]
    own = lambda i: jnp.minimum(i, steps - 1)
    other = lambda i: jnp.maximum(i - steps, 0)
    for _ in range(2):
        in_specs += [pl.BlockSpec((1, width, tile), lambda i: (0, 0, own(i))),
                     pl.BlockSpec((1, width, tile), lambda i: (0, 0, other(i)))]
    in_specs += [pl.BlockSpec((1, tile, width), lambda i: (0, own(i), 0)),
                 pl.BlockSpec((1, tile, width), lambda i: (0, other(i), 0))]
    rows = SUB * len(specs)
    outs = pl.pallas_call(
        partial(expert_kernel, specs=tuple(specs), steps=steps),
        grid=(2 * steps,),
        in_specs=in_specs,
        out_specs=out_specs,
        out_shape=out_shapes,
        scratch_shapes=[pltpu.VMEM((rows, width), bf16), pltpu.VMEM((rows, width), f32),
                        pltpu.VMEM((rows, LANES), f32), pltpu.VMEM((rows, LANES), f32)],
        compiler_params=pltpu.CompilerParams(
            dimension_semantics=("arbitrary",), vmem_limit_bytes=56 * 1024 * 1024),
        cost_estimate=pl.CostEstimate(
            flops=6 * rows * width * 2 * hidden, transcendentals=0,
            bytes_accessed=12 * width * hidden),
        interpret=INTERPRET,
        name="experts",
    )(where, *flat, weights[0], partner_weights[0], weights[1], partner_weights[1],
      weights[2], partner_weights[2])
    results, cursor = [], 0
    for subs, _ in specs:
        take = len(message_rows(subs, blocks))
        results.append(list(outs[cursor:cursor + take]))
        cursor += take
    return results


def message_rows(subs, blocks):
    first = SUB * blocks * (2 if subs == 4 else 1)
    second = SUB * blocks * min(subs - 1, 2)
    return [first, second] if second else [first]


def body(tokens, norm_gain, expert_ids, route_weight, gate_weight, up_weight, down_weight):
    devices = lax.axis_size("ep")
    ring = devices // 2
    experts = ring // 2
    rows, width = tokens.shape
    blocks = width // LANES
    capacity = min(rows, 2 * rows * expert_ids.shape[1] // experts)
    hops = ring // 2
    chip = lax.axis_index("ep") // 2
    where = jnp.stack([chip // 2, chip % 2]).astype(jnp.int32)
    subs_at = [4] + [
        min(rows, capacity * (experts // 2 - (k + 1) // 2 + 1)) // SUB for k in range(1, hops + 1)]

    swap = [(i, i ^ 1) for i in range(devices)]
    weights = (gate_weight, up_weight, down_weight)
    partner = tuple(lax.ppermute(w, "ep", swap) for w in weights)

    full = message_rows(4, blocks)
    shapes = [jax.ShapeDtypeStruct((full[0] + META, LANES), bf16),
              jax.ShapeDtypeStruct((full[1], LANES), bf16)]
    upa, upb, downa, downb, up_back, down_back = pl.pallas_call(
        partial(prepare_kernel, experts=experts),
        in_specs=[SMEM, VMEM, VMEM, VMEM, VMEM],
        out_specs=[VMEM] * 6,
        out_shape=shapes * 2 + [jax.ShapeDtypeStruct((rows, rows), bf16)] * 2,
        interpret=INTERPRET,
        name="prepare",
    )(where, tokens, norm_gain.reshape(1, width), expert_ids, route_weight)

    def cut(pair, subs, gap):
        sizes = message_rows(subs, blocks)
        if gap:
            sizes[0] += META
        return [x[:n] if x.shape[0] != n else x for x, n in zip(pair, sizes)]

    arrived = {(0, 0): [upa, upb]}
    moving = {1: [upa, upb], -1: [downa, downb]}
    for k in range(1, hops + 1):
        for way in (1, -1):
            moving[way] = [shifted(x, 2 * way) for x in cut(moving[way], subs_at[k], True)]
            arrived[way, k] = moving[way]

    given = {}
    edges = [0, 4, 8, 12, 14, 16]
    edges = [e * hops // 16 for e in edges]
    for low, high in zip(edges[:-1], edges[1:]):
        keys = [(0, 0)] if low == 0 else []
        keys += [(way, k) for k in range(low + 1, high + 1) for way in (1, -1)]
        specs = [(subs_at[k], None if k < hops else (1 if way == 1 else 0)) for way, k in keys]
        for key, value in zip(keys, apply_experts(where, [arrived[k] for k in keys], specs,
                                                  weights, partner)):
            given[key] = value

    totals = {way: given[way, hops] for way in (1, -1)}
    for k in range(hops - 1, -1, -1):
        for way in (1, -1):
            came = [shifted(x, -2 * way) for x in totals[way]]
            if k == 0:
                totals[way] = came
                continue
            mine = given[way, k]
            joined = []
            for number, value in enumerate(mine):
                if number < len(came):
                    more = came[number]
                    padded = jnp.pad(more, ((0, value.shape[0] - more.shape[0]), (0, 0)))
                    value = (value.astype(f32) + padded.astype(f32)).astype(bf16)
                joined.append(value)
            totals[way] = joined

    return pl.pallas_call(
        finish_kernel,
        in_specs=[VMEM] * 8,
        out_specs=VMEM,
        out_shape=jax.ShapeDtypeStruct((rows, width), bf16),
        interpret=INTERPRET,
        name="finish",
    )(*given[0, 0], *totals[1], *totals[-1], up_back, down_back)


def solution(mesh):
    placed = (
        P(("grp", "ep"), None),
        P(),
        P(("grp", "ep"), None),
        P(("grp", "ep"), None),
        P("ep", None, None),
        P("ep", None, None),
        P("ep", None, None),
    )
    return jax.shard_map(
        body, mesh=mesh, in_specs=placed, out_specs=P(("grp", "ep"), None), check_vma=False
    )
```

time: 717 us -> 440 us (0.61); the launches traced: 717 us -> 431 us
  waiting for transfers between devices: 392 us -> 123 us
  blocking collectives: 233 us -> 0 us
  starting transfers between devices: 7.96 us -> 223 us
  Pallas kernels: 0 us -> 68.8 us
  other arithmetic: 34.3 us -> 5.93 us
  matrix products: 22.5 us -> 0 us
  local copies, waits for them, and re-layouts: 26.5 us -> 7.99 us
    all_to_all x1 -> x0, blocking collectives: 233 us -> none  [body(): lax.all_to_all(pieces, 'ep', split_axis=0, concat_axis=0, tiled=True)]
    ppermute x4 -> x123, starting transfers between devices: 0.42 us -> 223 us  [the longest x120 223 us: shifted(): lax.ppermute(array, 'ep', [(i, (i + step) % size) for i in range(size)])]
    all_to_all x1 -> x0, waiting for transfers between devices: 199 us -> none  [body(): lax.all_to_all(finished, 'ep', split_axis=0, concat_axis=0, tiled=True)]
    ppermute x4 -> x123, waiting for transfers between devices: 193 us -> 123 us  [the longest x120 123 us: shifted(): lax.ppermute(array, 'ep', [(i, (i + step) % size) for i in range(size)])]
    pallas_call x0 -> x7, Pallas kernels: none -> 68.8 us  [the longest x5 63.2 us: apply_experts(): pl.pallas_call(partial(expert_kernel, specs=tuple(specs), steps=steps), g...]
    dot_general x2 -> x0, matrix products: 22.5 us -> none  [the longest x1 16.5 us: expert_rows(): jnp.einsum('scf,fd->scd', active, down_weight[0], preferred_element_type=...]
    select_n x6 -> x0, other arithmetic: 9.34 us -> none  [the longest x2 7.49 us: body(): first_half = jnp.where(upper_bit == 1, partner, gathered)]
    gather x3 -> x0, local copies, waits for them, and re-layouts: 9.24 us -> none  [the longest x2 5.89 us: body(): jnp.take(results, target, axis=0).reshape(tok_rows, top_count, width)]
  transfers between devices with their start and end apart: 5 -> 123, of which waited for: 5 -> 55; matrix products, arithmetic and copies ran while one was open for 0% -> 1% of each run, Pallas kernels for 0% -> 15%
where the time goes in v1:
time: 440 us; the launch traced here: 431 us
  starting transfers between devices  223 us (51%)
  waiting for transfers between devices  123 us (28%)
  Pallas kernels  68.8 us (16%)
  local copies, waits for them, and re-layouts  7.99 us (2%)
  other arithmetic  5.93 us (1%)
    ppermute x120, starting transfers between devices, shifted(): lax.ppermute(array, 'ep', [(i, (i + step) % size) for i in range(size)])  223 us
    ppermute x120, waiting for transfers between devices, shifted(): lax.ppermute(array, 'ep', [(i, (i + step) % size) for i in range(size)])  123 us
    pallas_call x5, Pallas kernels, apply_experts(): pl.pallas_call(partial(expert_kernel, specs=tuple(specs), steps=steps), g...  63.2 us
  transfers between devices with their start and end apart: 123, of which 55 were waited for; matrix products, arithmetic and copies ran while one was open for 1% of the time, Pallas kernels for 15%

profile of v1, /device:TPU:46, one launch (start us, length us, event | category | flops | bytes accessed | tf_op | source)
XLA Modules:
  0.0 431.4 jit_solution(13974986877925051985)
XLA Ops:
  10.7 19.0 %collective-permute-start.3 = (bf16[1024,128]{1,0:T(8,128)(2,1)}, bf16[1024,128]{1,0:T(8,128)(2,1)S(1)}, u32[]{:S(2)}, u32[]{:S(2)}) collective-permute-start(bf16[1024,128]{1,0:T(8,128)(2,1)} %get-tuple-element.76), channel_id=1, source_target_pairs={{0,62},{1,63},{2,0},{3,1},{4,2},{5,3},{6,4},{7,5},{8,6},{9,7},{10,... | collective-permute-start | bytes 786440 | tf_op jit(solution)/shard_map/ppermute | solution.py:23
  31.6 5.3 %collective-permute-done.refs_3_ = bf16[1040,128]{1,0:T(8,128)(2,1)S(1)} collective-permute-done((bf16[1040,128]{1,0:T(8,128)(2,1)}, bf16[1040,128]{1,0:T(8,128)(2,1)S(1)}, u32[]{:S(2)}, u32[]{:S(2)}) %collective-permute-start) | collective-permute-done | bytes 266272 | tf_op jit(solution)/shard_map/ppermute | solution.py:23
  36.9 5.6 %collective-permute-done.1.refs_4_ = bf16[1024,128]{1,0:T(8,128)(2,1)S(1)} collective-permute-done((bf16[1024,128]{1,0:T(8,128)(2,1)}, bf16[1024,128]{1,0:T(8,128)(2,1)S(1)}, u32[]{:S(2)}, u32[]{:S(2)}) %collective-permute-start.1) | collective-permute-done | bytes 262176 | tf_op jit(solution)/shard_map/ppermute | solution.py:23
  46.6 6.5 %collective-permute-done.5.refs_8_ = bf16[1024,128]{1,0:T(8,128)(2,1)S(1)} collective-permute-done((bf16[1024,128]{1,0:T(8,128)(2,1)S(1)}, bf16[1024,128]{1,0:T(8,128)(2,1)S(1)}, u32[]{:S(2)}, u32[]{:S(2)}) %collective-permute-start.5) | collective-permute-done | bytes 262176 | tf_op jit(solution)/shard_map/ppermute | solution.py:23
  59.2 4.3 collective-permute-done.9.refs_12_
  63.5 5.7 %collective-permute-done.8.refs_11_ = bf16[1040,128]{1,0:T(8,128)(2,1)S(1)} collective-permute-done((bf16[1040,128]{1,0:T(8,128)(2,1)S(1)}, bf16[1040,128]{1,0:T(8,128)(2,1)S(1)}, u32[]{:S(2)}, u32[]{:S(2)}) %collective-permute-start.8) | collective-permute-done | bytes 266272 | tf_op jit(solution)/shard_map/ppermute | solution.py:23
  74.9 4.5 %collective-permute-done.15.refs_18_ = bf16[1024,128]{1,0:T(8,128)(2,1)S(1)} collective-permute-done((bf16[1024,128]{1,0:T(8,128)(2,1)S(1)}, bf16[1024,128]{1,0:T(8,128)(2,1)S(1)}, u32[]{:S(2)}, u32[]{:S(2)}) %collective-permute-start.15) | collective-permute-done | bytes 262176 | tf_op jit(solution)/shard_map/ppermute | solution.py:23
  108.1 5.1 %collective-permute-done.30.refs_12_ = bf16[1024,128]{1,0:T(8,128)(2,1)S(1)} collective-permute-done((bf16[1024,128]{1,0:T(8,128)(2,1)S(1)}, bf16[1024,128]{1,0:T(8,128)(2,1)S(1)}, u32[]{:S(2)}, u32[]{:S(2)}) %collective-permute-start.30) | collective-permute-done | bytes 262176 | tf_op jit(solution)/shard_map/ppermute | solution.py:23
  158.5 3.8 collective-permute-start.42
  187.9 15.7 %experts.5 = (bf16[1024,128]{1,0:T(8,128)(2,1)}, bf16[1024,128]{1,0:T(8,128)(2,1)}, bf16[1024,128]{1,0:T(8,128)(2,1)}, bf16[1024,128]{1,0:T(8,128)(2,1)}, bf16[1...) custom-call(s32[2]{0:T(128)} %pad_add_fusion.where_ref.refs_0_, ...), custom_call_target="tpu_custom_call" | custom-call | flops 3623878656 | bytes 12582912 | tf_op jit(solution)/shard_map/experts/pallas_call | solution.py:231
  210.9 14.7 %experts.6 = (bf16[1024,128]{1,0:T(8,128)(2,1)}, bf16[1024,128]{1,0:T(8,128)(2,1)}, bf16[1024,128]{1,0:T(8,128)(2,1)}, bf16[1024,128]{1,0:T(8,128)(2,1)}, bf16[1...) custom-call(s32[2]{0:T(128)} %pad_add_fusion.where_ref.refs_0_, ...), custom_call_target="tpu_custom_call" | custom-call | flops 3221225472 | bytes 12582912 | tf_op jit(solution)/shard_map/experts/pallas_call | solution.py:231
  232.5 14.2 %experts.7 = (bf16[1024,128]{1,0:T(8,128)(2,1)}, bf16[1024,128]{1,0:T(8,128)(2,1)}, bf16[1024,128]{1,0:T(8,128)(2,1)}, bf16[1024,128]{1,0:T(8,128)(2,1)}, bf16[1...) custom-call(s32[2]{0:T(128)} %pad_add_fusion.where_ref.refs_0_, ...), custom_call_target="tpu_custom_call" | custom-call | flops 3221225472 | bytes 12582912 | tf_op jit(solution)/shard_map/experts/pallas_call | solution.py:231
  251.4 9.5 %experts.8 = (bf16[512,128]{1,0:T(8,128)(2,1)}, bf16[512,128]{1,0:T(8,128)(2,1)}, bf16[512,128]{1,0:T(8,128)(2,1)}, bf16[512,128]{1,0:T(8,128)(2,1)}, bf16[512,1...) custom-call(s32[2]{0:T(128)} %pad_add_fusion.where_ref.refs_0_, ...), custom_call_target="tpu_custom_call" | custom-call | flops 1610612736 | bytes 12582912 | tf_op jit(solution)/shard_map/experts/pallas_call | solution.py:231
  264.6 9.1 %experts.9 = (bf16[512,128]{1,0:T(8,128)(2,1)}, bf16[512,128]{1,0:T(8,128)(2,1)}, bf16[512,128]{1,0:T(8,128)(2,1)}, bf16[512,128]{1,0:T(8,128)(2,1)}) custom-call(s32[2]{0:T(128)} %pad_add_fusion.where_ref.refs_0_, bf16[528,128]{1,0:T(8,128)(2,1)} %copy-done.95, bf16[528,128]{1,0:T(8,128)(2,1)} %copy-done.96, bf16[528,128]{1,0:T(8,128)(2,1)} %copy-done.97, ...), custom_call_target="tpu_custom_call" | custom-call | flops 1610612736 | bytes 12582912 | tf_op jit(solution)/shard_map/experts/pallas_call | solution.py:231
  294.0 3.8 collective-permute-start.66
  307.7 5.2 %collective-permute-done.67 = bf16[512,128]{1,0:T(8,128)(2,1)S(1)} collective-permute-done((bf16[512,128]{1,0:T(8,128)(2,1)S(1)}, bf16[512,128]{1,0:T(8,128)(2,1)S(1)}, u32[]{:S(2)}, u32[]{:S(2)}) %collective-permute-start.67) | collective-permute-done | bytes 131104 | tf_op jit(solution)/shard_map/ppermute | solution.py:23
  312.9 3.8 collective-permute-start.68
  320.7 3.8 collective-permute-start.69
  327.2 3.8 collective-permute-start.84
  332.8 3.8 collective-permute-start.70
  338.4 4.0 collective-permute-start.85
  344.0 3.8 collective-permute-start.71
  349.6 3.8 collective-permute-start.86
  355.2 3.8 collective-permute-start.72
  360.9 3.8 collective-permute-start.87
  366.5 3.8 collective-permute-start.73
  372.1 3.8 collective-permute-start.88
  377.7 3.8 collective-permute-start.74
  383.3 3.8 collective-permute-start.89
  389.0 3.8 collective-permute-start.75
  400.0 3.8 collective-permute-start.76
  423.4 4.1 collective-permute-done.108.refs_4_
  (514 shorter events, 235.8 us)
Async XLA Ops:
  6.4 30.5 %collective-permute-start = (bf16[1040,128]{1,0:T(8,128)(2,1)}, bf16[1040,128]{1,0:T(8,128)(2,1)S(1)}, u32[]{:S(2)}, u32[]{:S(2)}) collective-permute-start(bf16[1040,128]{1,0:T(8,128)(2,1)} %get-tuple-element.73.refs_1_), channel_id=1, source_target_pairs={{0,2},{1,3},{2,4},{3,5},{4,6},{5,7},{6,8},{7,9},{8,10},{9,11},{10,... | collective-permute-start | bytes 798728 | tf_op jit(solution)/shard_map/ppermute | solution.py:23
  8.5 34.0 %collective-permute-start.1 = (bf16[1024,128]{1,0:T(8,128)(2,1)}, bf16[1024,128]{1,0:T(8,128)(2,1)S(1)}, u32[]{:S(2)}, u32[]{:S(2)}) collective-permute-start(bf16[1024,128]{1,0:T(8,128)(2,1)} %get-tuple-element.74.refs_2_), channel_id=1, source_target_pairs={{0,2},{1,3},{2,4},{3,5},{4,6},{5,7},{6,8},{7,9},{8,10},{9,11},{10,... | collective-permute-start | bytes 786440 | tf_op jit(solution)/shard_map/ppermute | solution.py:23
  10.7 31.9 %collective-permute-start.3 = (bf16[1024,128]{1,0:T(8,128)(2,1)}, bf16[1024,128]{1,0:T(8,128)(2,1)S(1)}, u32[]{:S(2)}, u32[]{:S(2)}) collective-permute-start(bf16[1024,128]{1,0:T(8,128)(2,1)} %get-tuple-element.76), channel_id=1, source_target_pairs={{0,62},{1,63},{2,0},{3,1},{4,2},{5,3},{6,4},{7,5},{8,6},{9,7},{10,... | collective-permute-start | bytes 786440 | tf_op jit(solution)/shard_map/ppermute | solution.py:23
  29.7 16.1 %collective-permute-start.2 = (bf16[1040,128]{1,0:T(8,128)(2,1)}, bf16[1040,128]{1,0:T(8,128)(2,1)S(1)}, u32[]{:S(2)}, u32[]{:S(2)}) collective-permute-start(bf16[1040,128]{1,0:T(8,128)(2,1)} %get-tuple-element.75), channel_id=1, source_target_pairs={{0,62},{1,63},{2,0},{3,1},{4,2},{5,3},{6,4},{7,5},{8,6},{9,7},{10,... | collective-permute-start | bytes 798728 | tf_op jit(solution)/shard_map/ppermute | solution.py:23
  36.9 16.2 %collective-permute-start.4 = (bf16[1040,128]{1,0:T(8,128)(2,1)S(1)}, bf16[1040,128]{1,0:T(8,128)(2,1)S(1)}, u32[]{:S(2)}, u32[]{:S(2)}) collective-permute-start(bf16[1040,128]{1,0:T(8,128)(2,1)S(1)} %collective-permute-done.refs_3_), channel_id=1, source_target_pairs={{0,2},{1,3},{2,4},{3,5},{4,6},{5,7},{6,8},{7,9},{8,10},{9,11},{10,... | collective-permute-start | bytes 798728 | tf_op jit(solution)/shard_map/ppermute | solution.py:23
  53.1 16.1 %collective-permute-start.8 = (bf16[1040,128]{1,0:T(8,128)(2,1)S(1)}, bf16[1040,128]{1,0:T(8,128)(2,1)S(1)}, u32[]{:S(2)}, u32[]{:S(2)}) collective-permute-start(bf16[1040,128]{1,0:T(8,128)(2,1)S(1)} %collective-permute-done.4.refs_7_), channel_id=1, source_target_pairs={{0,2},{1,3},{2,4},{3,5},{4,6},{5,7},{6,8},{7,9},{8,10},{9,11},{10,... | collective-permute-start | bytes 798728 | tf_op jit(solution)/shard_map/ppermute | solution.py:23
  53.3 16.3 %collective-permute-start.11 = (bf16[1024,128]{1,0:T(8,128)(2,1)S(1)}, bf16[1024,128]{1,0:T(8,128)(2,1)S(1)}, u32[]{:S(2)}, u32[]{:S(2)}) collective-permute-start(bf16[1024,128]{1,0:T(8,128)(2,1)S(1)} %collective-permute-done.7.refs_10_), channel_id=1, source_target_pairs={{0,62},{1,63},{2,0},{3,1},{4,2},{5,3},{6,4},{7,5},{8,6},{9,7},{10,... | collective-permute-start | bytes 786440 | tf_op jit(solution)/shard_map/ppermute | solution.py:23
  56.6 16.2 %collective-permute-start.10 = (bf16[1040,128]{1,0:T(8,128)(2,1)S(1)}, bf16[1040,128]{1,0:T(8,128)(2,1)S(1)}, u32[]{:S(2)}, u32[]{:S(2)}) collective-permute-start(bf16[1040,128]{1,0:T(8,128)(2,1)S(1)} %collective-permute-done.6.refs_9_), channel_id=1, source_target_pairs={{0,62},{1,63},{2,0},{3,1},{4,2},{5,3},{6,4},{7,5},{8,6},{9,7},{10,... | collective-permute-start | bytes 798728 | tf_op jit(solution)/shard_map/ppermute | solution.py:23
  74.8 14.1 %collective-permute-start.20 = (bf16[1024,128]{1,0:T(8,128)(2,1)S(1)}, bf16[1024,128]{1,0:T(8,128)(2,1)S(1)}, u32[]{:S(2)}, u32[]{:S(2)}) collective-permute-start(bf16[1024,128]{1,0:T(8,128)(2,1)S(1)} %collective-permute-done.13.refs_16_), channel_id=1, source_target_pairs={{0,2},{1,3},{2,4},{3,5},{4,6},{5,7},{6,8},{7,9},{8,10},{9,11},{10,... | collective-permute-start | bytes 786440 | tf_op jit(solution)/shard_map/ppermute | solution.py:23
  100.2 62.2 %collective-permute-start.16 = (bf16[1,2048,512]{2,1,0:T(8,128)(2,1)}, bf16[1,2048,512]{2,1,0:T(8,128)(2,1)S(1)}, u32[]{:S(2)}, u32[]{:S(2)}) collective-permute-start(bf16[1,2048,512]{2,1,0:T(8,128)(2,1)} %refs_5_.1), channel_id=1, source_target_pairs={{0,1},{1,0},{2,3},{3,2},{4,5},{5,4},{6,7},{7,6},{8,9},{9,8},{10,11... | collective-permute-start | bytes 6291464 | tf_op jit(solution)/shard_map/ppermute | solution.py:277
  100.5 62.0 %collective-permute-start.17 = (bf16[1,2048,512]{2,1,0:T(8,128)(2,1)}, bf16[1,2048,512]{2,1,0:T(8,128)(2,1)S(1)}, u32[]{:S(2)}, u32[]{:S(2)}) collective-permute-start(bf16[1,2048,512]{2,1,0:T(8,128)(2,1)} %refs_7_.1), channel_id=1, source_target_pairs={{0,1},{1,0},{2,3},{3,2},{4,5},{5,4},{6,7},{7,6},{8,9},{9,8},{10,11... | collective-permute-start | bytes 6291464 | tf_op jit(solution)/shard_map/ppermute | solution.py:277
  113.2 73.3 %collective-permute-start.18 = (bf16[1,512,2048]{2,1,0:T(8,128)(2,1)}, bf16[1,512,2048]{2,1,0:T(8,128)(2,1)S(1)}, u32[]{:S(2)}, u32[]{:S(2)}) collective-permute-start(bf16[1,512,2048]{2,1,0:T(8,128)(2,1)} %refs_9_.3), channel_id=1, source_target_pairs={{0,1},{1,0},{2,3},{3,2},{4,5},{5,4},{6,7},{7,6},{8,9},{9,8},{10,11... | collective-permute-start | bytes 6291464 | tf_op jit(solution)/shard_map/ppermute | solution.py:277
  176.9 30.5 %collective-permute-start.48 = (bf16[1024,128]{1,0:T(8,128)(2,1)}, bf16[1024,128]{1,0:T(8,128)(2,1)S(1)}, u32[]{:S(2)}, u32[]{:S(2)}) collective-permute-start(bf16[1024,128]{1,0:T(8,128)(2,1)} %collective-permute-done.44.refs_10_), channel_id=1, source_target_pairs={{0,2},{1,3},{2,4},{3,5},{4,6},{5,7},{6,8},{7,9},{8,10},{9,11},{10,... | collective-permute-start | bytes 786440 | tf_op jit(solution)/shard_map/ppermute | solution.py:23
  179.4 28.2 %collective-permute-start.50 = (bf16[1024,128]{1,0:T(8,128)(2,1)}, bf16[1024,128]{1,0:T(8,128)(2,1)S(1)}, u32[]{:S(2)}, u32[]{:S(2)}) collective-permute-start(bf16[1024,128]{1,0:T(8,128)(2,1)} %collective-permute-done.46.refs_12_), channel_id=1, source_target_pairs={{0,62},{1,63},{2,0},{3,1},{4,2},{5,3},{6,4},{7,5},{8,6},{9,7},{10,... | collective-permute-start | bytes 786440 | tf_op jit(solution)/shard_map/ppermute | solution.py:23
  183.2 20.4 %collective-permute-start.51 = (bf16[528,128]{1,0:T(8,128)(2,1)}, bf16[528,128]{1,0:T(8,128)(2,1)}, u32[]{:S(2)}, u32[]{:S(2)}) collective-permute-start(bf16[528,128]{1,0:T(8,128)(2,1)} %collective-permute-done.47.refs_13_), channel_id=1, source_target_pairs={{0,2},{1,3},{2,4},{3,5},{4,6},{5,7},{6,8},{7,9},{8,10},{9,11},{10,... | collective-permute-start | bytes 405512 | tf_op jit(solution)/shard_map/ppermute | solution.py:23
  183.2 21.0 %collective-permute-start.53 = (bf16[528,128]{1,0:T(8,128)(2,1)}, bf16[528,128]{1,0:T(8,128)(2,1)}, u32[]{:S(2)}, u32[]{:S(2)}) collective-permute-start(bf16[528,128]{1,0:T(8,128)(2,1)} %collective-permute-done.49.refs_15_), channel_id=1, source_target_pairs={{0,62},{1,63},{2,0},{3,1},{4,2},{5,3},{6,4},{7,5},{8,6},{9,7},{10,... | collective-permute-start | bytes 405512 | tf_op jit(solution)/shard_map/ppermute | solution.py:23
  203.7 22.0 %collective-permute-start.55 = (bf16[528,128]{1,0:T(8,128)(2,1)}, bf16[528,128]{1,0:T(8,128)(2,1)S(1)}, u32[]{:S(2)}, u32[]{:S(2)}) collective-permute-start(bf16[528,128]{1,0:T(8,128)(2,1)} %collective-permute-done.51.refs_1_), channel_id=1, source_target_pairs={{0,2},{1,3},{2,4},{3,5},{4,6},{5,7},{6,8},{7,9},{8,10},{9,11},{10,... | collective-permute-start | bytes 405512 | tf_op jit(solution)/shard_map/ppermute | solution.py:23
  204.2 21.6 %collective-permute-start.57 = (bf16[528,128]{1,0:T(8,128)(2,1)}, bf16[528,128]{1,0:T(8,128)(2,1)S(1)}, u32[]{:S(2)}, u32[]{:S(2)}) collective-permute-start(bf16[528,128]{1,0:T(8,128)(2,1)} %collective-permute-done.53.refs_3_), channel_id=1, source_target_pairs={{0,62},{1,63},{2,0},{3,1},{4,2},{5,3},{6,4},{7,5},{8,6},{9,7},{10,... | collective-permute-start | bytes 405512 | tf_op jit(solution)/shard_map/ppermute | solution.py:23
  207.5 21.6 %collective-permute-start.52 = (bf16[512,128]{1,0:T(8,128)(2,1)S(1)}, bf16[512,128]{1,0:T(8,128)(2,1)S(1)}, u32[]{:S(2)}, u32[]{:S(2)}) collective-permute-start(bf16[512,128]{1,0:T(8,128)(2,1)S(1)} %slice.18), channel_id=1, source_target_pairs={{0,2},{1,3},{2,4},{3,5},{4,6},{5,7},{6,8},{7,9},{8,10},{9,11},{10,... | collective-permute-start | bytes 393224 | tf_op jit(solution)/shard_map/ppermute | solution.py:23
  207.6 21.5 %collective-permute-start.54 = (bf16[512,128]{1,0:T(8,128)(2,1)S(1)}, bf16[512,128]{1,0:T(8,128)(2,1)S(1)}, u32[]{:S(2)}, u32[]{:S(2)}) collective-permute-start(bf16[512,128]{1,0:T(8,128)(2,1)S(1)} %slice.19), channel_id=1, source_target_pairs={{0,62},{1,63},{2,0},{3,1},{4,2},{5,3},{6,4},{7,5},{8,6},{9,7},{10,... | collective-permute-start | bytes 393224 | tf_op jit(solution)/shard_map/ppermute | solution.py:23
  225.7 21.0 %collective-permute-start.59 = (bf16[528,128]{1,0:T(8,128)(2,1)S(1)}, bf16[528,128]{1,0:T(8,128)(2,1)S(1)}, u32[]{:S(2)}, u32[]{:S(2)}) collective-permute-start(bf16[528,128]{1,0:T(8,128)(2,1)S(1)} %collective-permute-done.55.refs_5_), channel_id=1, source_target_pairs={{0,2},{1,3},{2,4},{3,5},{4,6},{5,7},{6,8},{7,9},{8,10},{9,11},{10,... | collective-permute-start | bytes 405512 | tf_op jit(solution)/shard_map/ppermute | solution.py:23
  225.9 21.0 %collective-permute-start.60 = (bf16[528,128]{1,0:T(8,128)(2,1)S(1)}, bf16[528,128]{1,0:T(8,128)(2,1)S(1)}, u32[]{:S(2)}, u32[]{:S(2)}) collective-permute-start(bf16[528,128]{1,0:T(8,128)(2,1)S(1)} %collective-permute-done.57.refs_7_), channel_id=1, source_target_pairs={{0,62},{1,63},{2,0},{3,1},{4,2},{5,3},{6,4},{7,5},{8,6},{9,7},{10,... | collective-permute-start | bytes 405512 | tf_op jit(solution)/shard_map/ppermute | solution.py:23
  229.1 21.0 %collective-permute-start.56 = (bf16[512,128]{1,0:T(8,128)(2,1)S(1)}, bf16[512,128]{1,0:T(8,128)(2,1)S(1)}, u32[]{:S(2)}, u32[]{:S(2)}) collective-permute-start(bf16[512,128]{1,0:T(8,128)(2,1)S(1)} %collective-permute-done.52.refs_2_), channel_id=1, source_target_pairs={{0,2},{1,3},{2,4},{3,5},{4,6},{5,7},{6,8},{7,9},{8,10},{9,11},{10,... | collective-permute-start | bytes 393224 | tf_op jit(solution)/shard_map/ppermute | solution.py:23
  229.1 21.0 %collective-permute-start.58 = (bf16[512,128]{1,0:T(8,128)(2,1)S(1)}, bf16[512,128]{1,0:T(8,128)(2,1)S(1)}, u32[]{:S(2)}, u32[]{:S(2)}) collective-permute-start(bf16[512,128]{1,0:T(8,128)(2,1)S(1)} %collective-permute-done.54.refs_4_), channel_id=1, source_target_pairs={{0,62},{1,63},{2,0},{3,1},{4,2},{5,3},{6,4},{7,5},{8,6},{9,7},{10,... | collective-permute-start | bytes 393224 | tf_op jit(solution)/shard_map/ppermute | solution.py:23
  246.7 16.6 %collective-permute-start.61 = (bf16[528,128]{1,0:T(8,128)(2,1)S(1)}, bf16[528,128]{1,0:T(8,128)(2,1)S(1)}, u32[]{:S(2)}, u32[]{:S(2)}) collective-permute-start(bf16[528,128]{1,0:T(8,128)(2,1)S(1)} %collective-permute-done.59.refs_1_), channel_id=1, source_target_pairs={{0,2},{1,3},{2,4},{3,5},{4,6},{5,7},{6,8},{7,9},{8,10},{9,11},{10,... | collective-permute-start | bytes 405512 | tf_op jit(solution)/shard_map/ppermute | solution.py:23
  246.9 16.4 %collective-permute-start.62 = (bf16[528,128]{1,0:T(8,128)(2,1)S(1)}, bf16[528,128]{1,0:T(8,128)(2,1)S(1)}, u32[]{:S(2)}, u32[]{:S(2)}) collective-permute-start(bf16[528,128]{1,0:T(8,128)(2,1)S(1)} %collective-permute-done.60.refs_2_), channel_id=1, source_target_pairs={{0,62},{1,63},{2,0},{3,1},{4,2},{5,3},{6,4},{7,5},{8,6},{9,7},{10,... | collective-permute-start | bytes 405512 | tf_op jit(solution)/shard_map/ppermute | solution.py:23
  260.9 14.9 %collective-permute-start.79 = (bf16[512,128]{1,0:T(8,128)(2,1)}, bf16[512,128]{1,0:T(8,128)(2,1)S(1)}, u32[]{:S(2)}, u32[]{:S(2)}) collective-permute-start(bf16[512,128]{1,0:T(8,128)(2,1)} %get-tuple-element.108), channel_id=1, source_target_pairs={{0,62},{1,63},{2,0},{3,1},{4,2},{5,3},{6,4},{7,5},{8,6},{9,7},{10,... | collective-permute-start | bytes 393224 | tf_op jit(solution)/shard_map/ppermute | solution.py:23
  261.1 17.5 %collective-permute-start.109 = (bf16[512,128]{1,0:T(8,128)(2,1)}, bf16[512,128]{1,0:T(8,128)(2,1)S(1)}, u32[]{:S(2)}, u32[]{:S(2)}) collective-permute-start(bf16[512,128]{1,0:T(8,128)(2,1)} %get-tuple-element.138), channel_id=1, source_target_pairs={{0,2},{1,3},{2,4},{3,5},{4,6},{5,7},{6,8},{7,9},{8,10},{9,11},{10,... | collective-permute-start | bytes 393224 | tf_op jit(solution)/shard_map/ppermute | solution.py:23
  284.2 15.7 %collective-permute-start.81 = (bf16[1024,128]{1,0:T(8,128)(2,1)S(1)}, bf16[1024,128]{1,0:T(8,128)(2,1)S(1)}, u32[]{:S(2)}, u32[]{:S(2)}) collective-permute-start(bf16[1024,128]{1,0:T(8,128)(2,1)S(1)} %add_convert_fusion.33), channel_id=1, source_target_pairs={{0,62},{1,63},{2,0},{3,1},{4,2},{5,3},{6,4},{7,5},{8,6},{9,7},{10,... | collective-permute-start | bytes 786440 | tf_op jit(solution)/shard_map/ppermute | solution.py:23
  287.6 15.8 %collective-permute-start.111 = (bf16[1024,128]{1,0:T(8,128)(2,1)S(1)}, bf16[1024,128]{1,0:T(8,128)(2,1)S(1)}, u32[]{:S(2)}, u32[]{:S(2)}) collective-permute-start(bf16[1024,128]{1,0:T(8,128)(2,1)S(1)} %add_convert_fusion.11), channel_id=1, source_target_pairs={{0,2},{1,3},{2,4},{3,5},{4,6},{5,7},{6,8},{7,9},{8,10},{9,11},{10,... | collective-permute-start | bytes 786440 | tf_op jit(solution)/shard_map/ppermute | solution.py:23
  300.1 16.9 %collective-permute-start.82 = (bf16[1024,128]{1,0:T(8,128)(2,1)S(1)}, bf16[1024,128]{1,0:T(8,128)(2,1)S(1)}, u32[]{:S(2)}, u32[]{:S(2)}) collective-permute-start(bf16[1024,128]{1,0:T(8,128)(2,1)S(1)} %add_convert_fusion.32), channel_id=1, source_target_pairs={{0,62},{1,63},{2,0},{3,1},{4,2},{5,3},{6,4},{7,5},{8,6},{9,7},{10,... | collective-permute-start | bytes 786440 | tf_op jit(solution)/shard_map/ppermute | solution.py:23
  303.5 16.9 %collective-permute-start.112 = (bf16[1024,128]{1,0:T(8,128)(2,1)S(1)}, bf16[1024,128]{1,0:T(8,128)(2,1)S(1)}, u32[]{:S(2)}, u32[]{:S(2)}) collective-permute-start(bf16[1024,128]{1,0:T(8,128)(2,1)S(1)} %add_convert_fusion.10), channel_id=1, source_target_pairs={{0,2},{1,3},{2,4},{3,5},{4,6},{5,7},{6,8},{7,9},{8,10},{9,11},{10,... | collective-permute-start | bytes 786440 | tf_op jit(solution)/shard_map/ppermute | solution.py:23
  (206 other events, 3977.0 us)

commit v2 on v1

--- a/solution.py
+++ b/solution.py
@@ -7,9 +7,11 @@
 from jax.experimental.pallas import tpu as pltpu
 from jax.sharding import PartitionSpec as P
 
+
 INTERPRET = False
 LANES = 128
 SUB = 32
+STRIDE = 2
 META = 16
 EPSILON = 1e-05
 clamp_limit = 7.0
@@ -99,7 +101,7 @@
         ref[start + SUB * c:start + SUB * (c + 1), :] = rows[:, LANES * c:LANES * (c + 1)]
 
 
-def get_block(refs, subs, blocks, gap, c, axis=0):
+def get_block(refs, subs, blocks, gap, c):
     parts = []
     for sub in range(subs):
         which, start = sub_place(sub, blocks, gap)
@@ -108,7 +110,6 @@
 
 
 def expert_kernel(*refs, specs, steps):
-    count = len(specs)
     where_ref = refs[0]
     cursor = 1
     sources = []
@@ -158,26 +159,21 @@
                     hot, get_block(sources[number], subs, blocks, META, c),
                     preferred_element_type=f32).astype(bf16)
 
-    def partial_sum(gate_ref, up_ref, down_ref):
-        rows = rows_ref[...]
-        gate = jnp.minimum(jnp.dot(rows, gate_ref[0], preferred_element_type=f32), clamp_limit)
-        up = jnp.clip(jnp.dot(rows, up_ref[0], preferred_element_type=f32), -clamp_limit, clamp_limit)
-        active = ((up + 1.0) * (gate * jax.nn.sigmoid(gate * sigmoid_slope))).astype(bf16)
-        return jnp.dot(active, down_ref[0], preferred_element_type=f32)
-
-    @pl.when(step == 0)
-    def _():
-        sum_ref[...] = partial_sum(gates[0], ups[0], downs[0])
-
-    @pl.when((step > 0) & (step < steps))
-    def _():
-        sum_ref[...] += partial_sum(gates[0], ups[0], downs[0])
-
-    @pl.when(step >= steps)
-    def _():
-        sum_ref[...] += partial_sum(gates[1], ups[1], downs[1])
-
-    @pl.when(step == 2 * steps - 1)
+    rows = rows_ref[...]
+    tile = gates[0].shape[2]
+    actives = []
+    for gate_ref, up_ref in zip(gates, ups):
+        both = jnp.dot(rows, jnp.concatenate([gate_ref[0], up_ref[0]], axis=1),
+                       preferred_element_type=f32)
+        gate = jnp.minimum(both[:, :tile], clamp_limit)
+        up = jnp.clip(both[:, tile:], -clamp_limit, clamp_limit)
+        actives.append(((up + 1.0) * (gate * jax.nn.sigmoid(gate * sigmoid_slope))).astype(bf16))
+    part = jnp.dot(jnp.concatenate(actives, axis=1),
+                   jnp.concatenate([downs[0][0], downs[1][0]], axis=0),
+                   preferred_element_type=f32)
+    sum_ref[...] = jnp.where(step == 0, 0.0, sum_ref[...]) + part
+
+    @pl.when(step == steps - 1)
     def _():
         for number, (subs, _) in enumerate(specs):
             span = pl.ds(SUB * number, SUB)
@@ -209,7 +205,7 @@
 def apply_experts(where, sources, specs, weights, partner_weights):
     width = weights[0].shape[1]
     hidden = weights[0].shape[2]
-    tile = min(256, hidden)
+    tile = min(LANES, hidden)
     steps = hidden // tile
     blocks = width // LANES
     flat, out_shapes, in_specs, out_specs = [], [], [SMEM], []
@@ -220,17 +216,12 @@
         sizes = message_rows(subs, blocks)
         out_shapes += [jax.ShapeDtypeStruct((n, LANES), bf16) for n in sizes]
         out_specs += [held((n, LANES)) for n in sizes]
-    own = lambda i: jnp.minimum(i, steps - 1)
-    other = lambda i: jnp.maximum(i - steps, 0)
-    for _ in range(2):
-        in_specs += [pl.BlockSpec((1, width, tile), lambda i: (0, 0, own(i))),
-                     pl.BlockSpec((1, width, tile), lambda i: (0, 0, other(i)))]
-    in_specs += [pl.BlockSpec((1, tile, width), lambda i: (0, own(i), 0)),
-                 pl.BlockSpec((1, tile, width), lambda i: (0, other(i), 0))]
+    in_specs += [pl.BlockSpec((1, width, tile), lambda i: (0, 0, i))] * 4
+    in_specs += [pl.BlockSpec((1, tile, width), lambda i: (0, i, 0))] * 2
     rows = SUB * len(specs)
     outs = pl.pallas_call(
         partial(expert_kernel, specs=tuple(specs), steps=steps),
-        grid=(2 * steps,),
+        grid=(steps,),
         in_specs=in_specs,
         out_specs=out_specs,
         out_shape=out_shapes,
@@ -259,7 +250,7 @@
     return [first, second] if second else [first]
 
 
-def body(tokens, norm_gain, expert_ids, route_weight, gate_weight, up_weight, down_weight):
+def layer(tokens, norm_gain, expert_ids, route_weight, gate_weight, up_weight, down_weight):
     devices = lax.axis_size("ep")
     ring = devices // 2
     experts = ring // 2
@@ -298,24 +289,23 @@
     moving = {1: [upa, upb], -1: [downa, downb]}
     for k in range(1, hops + 1):
         for way in (1, -1):
-            moving[way] = [shifted(x, 2 * way) for x in cut(moving[way], subs_at[k], True)]
+            moving[way] = [shifted(x, 2 * way)
+                           for x in cut(moving[way], subs_at[k], True)]
             arrived[way, k] = moving[way]
 
     given = {}
-    edges = [0, 4, 8, 12, 14, 16]
-    edges = [e * hops // 16 for e in edges]
-    for low, high in zip(edges[:-1], edges[1:]):
+    for low in range(0, hops, STRIDE):
         keys = [(0, 0)] if low == 0 else []
-        keys += [(way, k) for k in range(low + 1, high + 1) for way in (1, -1)]
+        keys += [(way, k) for k in range(low + 1, low + STRIDE + 1) for way in (1, -1)]
         specs = [(subs_at[k], None if k < hops else (1 if way == 1 else 0)) for way, k in keys]
-        for key, value in zip(keys, apply_experts(where, [arrived[k] for k in keys], specs,
-                                                  weights, partner)):
-            given[key] = value
+        values = apply_experts(where, [arrived[k] for k in keys], specs, weights, partner)
+        given.update(zip(keys, values))
 
     totals = {way: given[way, hops] for way in (1, -1)}
     for k in range(hops - 1, -1, -1):
         for way in (1, -1):
-            came = [shifted(x, -2 * way) for x in totals[way]]
+            came = [shifted(x, -2 * way)
+                    for x in totals[way]]
             if k == 0:
                 totals[way] = came
                 continue
@@ -350,5 +340,5 @@
         P("ep", None, None),
     )
     return jax.shard_map(
-        body, mesh=mesh, in_specs=placed, out_specs=P(("grp", "ep"), None), check_vma=False
+        layer, mesh=mesh, in_specs=placed, out_specs=P(("grp", "ep"), None), check_vma=False
     )

time: 440 us -> 448 us (1.018)
  Pallas kernels: 68.8 us -> 88.8 us
  waiting for transfers between devices: 123 us -> 112 us
    pallas_call x5 -> x8, Pallas kernels: 63.2 us -> 83.2 us  [apply_experts(): pl.pallas_call(partial(expert_kernel, specs=tuple(specs), steps=steps), g...]
    ppermute x120, waiting for transfers between devices: 123 us -> 112 us  [shifted(): lax.ppermute(array, 'ep', [(i, (i + step) % size) for i in range(size)])]
  transfers between devices with their start and end apart: 123 -> 123, of which waited for: 55 -> 65; matrix products, arithmetic and copies ran while one was open for 1% -> 1% of each run, Pallas kernels for 15% -> 19%
where the time goes in v2:
time: 448 us; the launch traced here: 439 us
  starting transfers between devices  222 us (50%)
  waiting for transfers between devices  112 us (25%)
  Pallas kernels  88.8 us (20%)
  local copies, waits for them, and re-layouts  7.94 us (2%)
  other arithmetic  5.96 us (1%)
    ppermute x120, starting transfers between devices, shifted(): lax.ppermute(array, 'ep', [(i, (i + step) % size) for i in range(size)])  222 us
    ppermute x120, waiting for transfers between devices, shifted(): lax.ppermute(array, 'ep', [(i, (i + step) % size) for i in range(size)])  112 us
    pallas_call x8, Pallas kernels, apply_experts(): pl.pallas_call(partial(expert_kernel, specs=tuple(specs), steps=steps), g...  83.2 us
  transfers between devices with their start and end apart: 123, of which 65 were waited for; matrix products, arithmetic and copies ran while one was open for 1% of the time, Pallas kernels for 19%

profile of v2, /device:TPU:46, one launch (start us, length us, event | category | flops | bytes accessed | tf_op | source)
XLA Modules:
  0.0 438.8 jit_solution(11187374198973527257)
XLA Ops:
  10.6 19.1 %collective-permute-start.3 = (bf16[1024,128]{1,0:T(8,128)(2,1)}, bf16[1024,128]{1,0:T(8,128)(2,1)S(1)}, u32[]{:S(2)}, u32[]{:S(2)}) collective-permute-start(bf16[1024,128]{1,0:T(8,128)(2,1)} %get-tuple-element.76), channel_id=1, source_target_pairs={{0,62},{1,63},{2,0},{3,1},{4,2},{5,3},{6,4},{7,5},{8,6},{9,7},{10,... | collective-permute-start | bytes 786440 | tf_op jit(solution)/shard_map/ppermute | solution.py:25
  31.6 5.2 %collective-permute-done.1.refs_4_ = bf16[1024,128]{1,0:T(8,128)(2,1)S(1)} collective-permute-done((bf16[1024,128]{1,0:T(8,128)(2,1)}, bf16[1024,128]{1,0:T(8,128)(2,1)S(1)}, u32[]{:S(2)}, u32[]{:S(2)}) %collective-permute-start.1) | collective-permute-done | bytes 262176 | tf_op jit(solution)/shard_map/ppermute | solution.py:25
  36.8 5.7 %collective-permute-done.refs_3_ = bf16[1040,128]{1,0:T(8,128)(2,1)S(1)} collective-permute-done((bf16[1040,128]{1,0:T(8,128)(2,1)}, bf16[1040,128]{1,0:T(8,128)(2,1)S(1)}, u32[]{:S(2)}, u32[]{:S(2)}) %collective-permute-start) | collective-permute-done | bytes 266272 | tf_op jit(solution)/shard_map/ppermute | solution.py:25
  48.1 4.3 collective-permute-done.7.refs_10_
  67.9 7.0 %collective-permute-done.16.refs_6_ = bf16[1024,128]{1,0:T(8,128)(2,1)S(1)} collective-permute-done((bf16[1024,128]{1,0:T(8,128)(2,1)S(1)}, bf16[1024,128]{1,0:T(8,128)(2,1)S(1)}, u32[]{:S(2)}, u32[]{:S(2)}) %collective-permute-start.16) | collective-permute-done | bytes 262176 | tf_op jit(solution)/shard_map/ppermute | solution.py:25
  95.0 4.1 collective-permute-done.24.refs_6_
  102.6 4.2 collective-permute-done.23.refs_5_
  110.3 4.8 %collective-permute-done.28.refs_2_ = bf16[1024,128]{1,0:T(8,128)(2,1)S(1)} collective-permute-done((bf16[1024,128]{1,0:T(8,128)(2,1)S(1)}, bf16[1024,128]{1,0:T(8,128)(2,1)S(1)}, u32[]{:S(2)}, u32[]{:S(2)}) %collective-permute-start.28) | collective-permute-done | bytes 262176 | tf_op jit(solution)/shard_map/ppermute | solution.py:25
  118.8 5.6 %collective-permute-done.27.refs_1_ = bf16[1040,128]{1,0:T(8,128)(2,1)S(1)} collective-permute-done((bf16[1040,128]{1,0:T(8,128)(2,1)S(1)}, bf16[1040,128]{1,0:T(8,128)(2,1)S(1)}, u32[]{:S(2)}, u32[]{:S(2)}) %collective-permute-start.27) | collective-permute-done | bytes 266272 | tf_op jit(solution)/shard_map/ppermute | solution.py:25
  157.5 4.2 collective-permute-start.46
  163.1 11.6 %experts.8 = (bf16[1024,128]{1,0:T(8,128)(2,1)}, bf16[1024,128]{1,0:T(8,128)(2,1)}, bf16[1024,128]{1,0:T(8,128)(2,1)}, bf16[1024,128]{1,0:T(8,128)(2,1)}, bf16[1...) custom-call(s32[2]{0:T(128)} %pad_add_fusion.where_ref.refs_0_, ...), custom_call_target="tpu_custom_call" | custom-call | flops 2013265920 | bytes 12582912 | tf_op jit(solution)/shard_map/experts/pallas_call | solution.py:222
  178.3 10.8 %experts.10 = (bf16[1024,128]{1,0:T(8,128)(2,1)}, bf16[1024,128]{1,0:T(8,128)(2,1)}, bf16[1024,128]{1,0:T(8,128)(2,1)}, bf16[1024,128]{1,0:T(8,128)(2,1)}, bf16[...) custom-call(s32[2]{0:T(128)} %pad_add_fusion.where_ref.refs_0_, ...), custom_call_target="tpu_custom_call" | custom-call | flops 1610612736 | bytes 12582912 | tf_op jit(solution)/shard_map/experts/pallas_call | solution.py:222
  195.7 10.7 %experts.9 = (bf16[1024,128]{1,0:T(8,128)(2,1)}, bf16[1024,128]{1,0:T(8,128)(2,1)}, bf16[1024,128]{1,0:T(8,128)(2,1)}, bf16[1024,128]{1,0:T(8,128)(2,1)}, bf16[1...) custom-call(s32[2]{0:T(128)} %pad_add_fusion.where_ref.refs_0_, ...), custom_call_target="tpu_custom_call" | custom-call | flops 1610612736 | bytes 12582912 | tf_op jit(solution)/shard_map/experts/pallas_call | solution.py:222
  210.0 10.7 %experts.11 = (bf16[1024,128]{1,0:T(8,128)(2,1)}, bf16[1024,128]{1,0:T(8,128)(2,1)}, bf16[1024,128]{1,0:T(8,128)(2,1)}, bf16[1024,128]{1,0:T(8,128)(2,1)}, bf16[...) custom-call(s32[2]{0:T(128)} %pad_add_fusion.where_ref.refs_0_, ...), custom_call_target="tpu_custom_call" | custom-call | flops 1610612736 | bytes 12582912 | tf_op jit(solution)/shard_map/experts/pallas_call | solution.py:222
  227.6 10.7 %experts.12 = (bf16[1024,128]{1,0:T(8,128)(2,1)}, bf16[1024,128]{1,0:T(8,128)(2,1)}, bf16[1024,128]{1,0:T(8,128)(2,1)}, bf16[1024,128]{1,0:T(8,128)(2,1)}, bf16[...) custom-call(s32[2]{0:T(128)} %pad_add_fusion.where_ref.refs_0_, ...), custom_call_target="tpu_custom_call" | custom-call | flops 1610612736 | bytes 12582912 | tf_op jit(solution)/shard_map/experts/pallas_call | solution.py:222
  245.2 10.1 %experts.13 = (bf16[512,128]{1,0:T(8,128)(2,1)}, bf16[1024,128]{1,0:T(8,128)(2,1)}, bf16[512,128]{1,0:T(8,128)(2,1)}, bf16[1024,128]{1,0:T(8,128)(2,1)}, bf16[51...) custom-call(s32[2]{0:T(128)} %pad_add_fusion.where_ref.refs_0_, ...), custom_call_target="tpu_custom_call" | custom-call | flops 1610612736 | bytes 12582912 | tf_op jit(solution)/shard_map/experts/pallas_call | solution.py:222
  260.1 9.6 %experts.14 = (bf16[512,128]{1,0:T(8,128)(2,1)}, bf16[512,128]{1,0:T(8,128)(2,1)}, bf16[512,128]{1,0:T(8,128)(2,1)}, bf16[512,128]{1,0:T(8,128)(2,1)}, bf16[512,...) custom-call(s32[2]{0:T(128)} %pad_add_fusion.where_ref.refs_0_, ...), custom_call_target="tpu_custom_call" | custom-call | flops 1610612736 | bytes 12582912 | tf_op jit(solution)/shard_map/experts/pallas_call | solution.py:222
  273.2 9.0 %experts.15 = (bf16[512,128]{1,0:T(8,128)(2,1)}, bf16[512,128]{1,0:T(8,128)(2,1)}, bf16[512,128]{1,0:T(8,128)(2,1)}, bf16[512,128]{1,0:T(8,128)(2,1)}) custom-call(s32[2]{0:T(128)} %pad_add_fusion.where_ref.refs_0_, bf16[528,128]{1,0:T(8,128)(2,1)} %copy-done.93, bf16[528,128]{1,0:T(8,128)(2,1)} %copy-done.94, bf16[528,128]{1,0:T(8,128)(2,1)} %copy-done.95, ...), custom_call_target="tpu_custom_call" | custom-call | flops 1610612736 | bytes 12582912 | tf_op jit(solution)/shard_map/experts/pallas_call | solution.py:222
  300.5 4.5 %collective-permute-done.65 = bf16[512,128]{1,0:T(8,128)(2,1)S(1)} collective-permute-done((bf16[512,128]{1,0:T(8,128)(2,1)S(1)}, bf16[512,128]{1,0:T(8,128)(2,1)S(1)}, u32[]{:S(2)}, u32[]{:S(2)}) %collective-permute-start.65) | collective-permute-done | bytes 131104 | tf_op jit(solution)/shard_map/ppermute | solution.py:25
  305.0 3.8 collective-permute-start.66
  316.8 5.2 %collective-permute-done.67 = bf16[512,128]{1,0:T(8,128)(2,1)S(1)} collective-permute-done((bf16[512,128]{1,0:T(8,128)(2,1)S(1)}, bf16[512,128]{1,0:T(8,128)(2,1)S(1)}, u32[]{:S(2)}, u32[]{:S(2)}) %collective-permute-start.67) | collective-permute-done | bytes 131104 | tf_op jit(solution)/shard_map/ppermute | solution.py:25
  322.1 3.8 collective-permute-start.68
  336.3 3.8 collective-permute-start.84
  341.9 3.8 collective-permute-start.70
  347.5 3.8 collective-permute-start.85
  353.2 3.8 collective-permute-start.71
  358.8 3.8 collective-permute-start.86
  364.4 3.8 collective-permute-start.72
  370.0 3.8 collective-permute-start.87
  375.6 3.8 collective-permute-start.73
  386.9 3.8 collective-permute-start.74
  427.4 3.9 collective-permute-done.122.refs_5_
  (517 shorter events, 233.6 us)
Async XLA Ops:
  6.4 30.4 %collective-permute-start.1 = (bf16[1024,128]{1,0:T(8,128)(2,1)}, bf16[1024,128]{1,0:T(8,128)(2,1)S(1)}, u32[]{:S(2)}, u32[]{:S(2)}) collective-permute-start(bf16[1024,128]{1,0:T(8,128)(2,1)} %get-tuple-element.74.refs_2_), channel_id=1, source_target_pairs={{0,2},{1,3},{2,4},{3,5},{4,6},{5,7},{6,8},{7,9},{8,10},{9,11},{10,... | collective-permute-start | bytes 786440 | tf_op jit(solution)/shard_map/ppermute | solution.py:25
  8.5 34.0 %collective-permute-start = (bf16[1040,128]{1,0:T(8,128)(2,1)}, bf16[1040,128]{1,0:T(8,128)(2,1)S(1)}, u32[]{:S(2)}, u32[]{:S(2)}) collective-permute-start(bf16[1040,128]{1,0:T(8,128)(2,1)} %get-tuple-element.73.refs_1_), channel_id=1, source_target_pairs={{0,2},{1,3},{2,4},{3,5},{4,6},{5,7},{6,8},{7,9},{8,10},{9,11},{10,... | collective-permute-start | bytes 798728 | tf_op jit(solution)/shard_map/ppermute | solution.py:25
  10.6 31.9 %collective-permute-start.3 = (bf16[1024,128]{1,0:T(8,128)(2,1)}, bf16[1024,128]{1,0:T(8,128)(2,1)S(1)}, u32[]{:S(2)}, u32[]{:S(2)}) collective-permute-start(bf16[1024,128]{1,0:T(8,128)(2,1)} %get-tuple-element.76), channel_id=1, source_target_pairs={{0,62},{1,63},{2,0},{3,1},{4,2},{5,3},{6,4},{7,5},{8,6},{9,7},{10,... | collective-permute-start | bytes 786440 | tf_op jit(solution)/shard_map/ppermute | solution.py:25
  29.7 16.1 %collective-permute-start.2 = (bf16[1040,128]{1,0:T(8,128)(2,1)}, bf16[1040,128]{1,0:T(8,128)(2,1)S(1)}, u32[]{:S(2)}, u32[]{:S(2)}) collective-permute-start(bf16[1040,128]{1,0:T(8,128)(2,1)} %get-tuple-element.75), channel_id=1, source_target_pairs={{0,62},{1,63},{2,0},{3,1},{4,2},{5,3},{6,4},{7,5},{8,6},{9,7},{10,... | collective-permute-start | bytes 798728 | tf_op jit(solution)/shard_map/ppermute | solution.py:25
  61.8 66.7 %collective-permute-start.8 = (bf16[1,2048,512]{2,1,0:T(8,128)(2,1)}, bf16[1,2048,512]{2,1,0:T(8,128)(2,1)S(1)}, u32[]{:S(2)}, u32[]{:S(2)}) collective-permute-start(bf16[1,2048,512]{2,1,0:T(8,128)(2,1)} %refs_5_.1), channel_id=1, source_target_pairs={{0,1},{1,0},{2,3},{3,2},{4,5},{5,4},{6,7},{7,6},{8,9},{9,8},{10,11... | collective-permute-start | bytes 6291464 | tf_op jit(solution)/shard_map/ppermute | solution.py:268
  61.8 66.9 %collective-permute-start.9 = (bf16[1,2048,512]{2,1,0:T(8,128)(2,1)}, bf16[1,2048,512]{2,1,0:T(8,128)(2,1)S(1)}, u32[]{:S(2)}, u32[]{:S(2)}) collective-permute-start(bf16[1,2048,512]{2,1,0:T(8,128)(2,1)} %refs_7_.1), channel_id=1, source_target_pairs={{0,1},{1,0},{2,3},{3,2},{4,5},{5,4},{6,7},{7,6},{8,9},{9,8},{10,11... | collective-permute-start | bytes 6291464 | tf_op jit(solution)/shard_map/ppermute | solution.py:268
  89.3 72.5 %collective-permute-start.10 = (bf16[1,512,2048]{2,1,0:T(8,128)(2,1)}, bf16[1,512,2048]{2,1,0:T(8,128)(2,1)S(1)}, u32[]{:S(2)}, u32[]{:S(2)}) collective-permute-start(bf16[1,512,2048]{2,1,0:T(8,128)(2,1)} %refs_9_.13), channel_id=1, source_target_pairs={{0,1},{1,0},{2,3},{3,2},{4,5},{5,4},{6,7},{7,6},{8,9},{9,8},{10,11... | collective-permute-start | bytes 6291464 | tf_op jit(solution)/shard_map/ppermute | solution.py:268
  152.0 22.8 %collective-permute-start.39 = (bf16[1040,128]{1,0:T(8,128)(2,1)}, bf16[1040,128]{1,0:T(8,128)(2,1)S(1)}, u32[]{:S(2)}, u32[]{:S(2)}) collective-permute-start(bf16[1040,128]{1,0:T(8,128)(2,1)} %collective-permute-done.35.refs_1_), channel_id=1, source_target_pairs={{0,2},{1,3},{2,4},{3,5},{4,6},{5,7},{6,8},{7,9},{8,10},{9,11},{10,... | collective-permute-start | bytes 798728 | tf_op jit(solution)/shard_map/ppermute | solution.py:25
  152.3 22.6 %collective-permute-start.41 = (bf16[1040,128]{1,0:T(8,128)(2,1)}, bf16[1040,128]{1,0:T(8,128)(2,1)S(1)}, u32[]{:S(2)}, u32[]{:S(2)}) collective-permute-start(bf16[1040,128]{1,0:T(8,128)(2,1)} %collective-permute-done.37.refs_3_), channel_id=1, source_target_pairs={{0,62},{1,63},{2,0},{3,1},{4,2},{5,3},{6,4},{7,5},{8,6},{9,7},{10,... | collective-permute-start | bytes 798728 | tf_op jit(solution)/shard_map/ppermute | solution.py:25
  157.5 35.0 %collective-permute-start.44 = (bf16[1024,128]{1,0:T(8,128)(2,1)}, bf16[1024,128]{1,0:T(8,128)(2,1)}, u32[]{:S(2)}, u32[]{:S(2)}) collective-permute-start(bf16[1024,128]{1,0:T(8,128)(2,1)} %collective-permute-done.40.refs_6_), channel_id=1, source_target_pairs={{0,2},{1,3},{2,4},{3,5},{4,6},{5,7},{6,8},{7,9},{8,10},{9,11},{10,... | collective-permute-start | bytes 786440 | tf_op jit(solution)/shard_map/ppermute | solution.py:25
  157.5 35.0 %collective-permute-start.46 = (bf16[1024,128]{1,0:T(8,128)(2,1)}, bf16[1024,128]{1,0:T(8,128)(2,1)}, u32[]{:S(2)}, u32[]{:S(2)}) collective-permute-start(bf16[1024,128]{1,0:T(8,128)(2,1)} %collective-permute-done.42.refs_8_), channel_id=1, source_target_pairs={{0,62},{1,63},{2,0},{3,1},{4,2},{5,3},{6,4},{7,5},{8,6},{9,7},{10,... | collective-permute-start | bytes 786440 | tf_op jit(solution)/shard_map/ppermute | solution.py:25
  189.1 17.3 %collective-permute-start.47 = (bf16[528,128]{1,0:T(8,128)(2,1)S(1)}, bf16[528,128]{1,0:T(8,128)(2,1)S(1)}, u32[]{:S(2)}, u32[]{:S(2)}) collective-permute-start(bf16[528,128]{1,0:T(8,128)(2,1)S(1)} %collective-permute-done.43.refs_1_), channel_id=1, source_target_pairs={{0,2},{1,3},{2,4},{3,5},{4,6},{5,7},{6,8},{7,9},{8,10},{9,11},{10,... | collective-permute-start | bytes 405512 | tf_op jit(solution)/shard_map/ppermute | solution.py:25
  189.3 17.3 %collective-permute-start.49 = (bf16[528,128]{1,0:T(8,128)(2,1)S(1)}, bf16[528,128]{1,0:T(8,128)(2,1)S(1)}, u32[]{:S(2)}, u32[]{:S(2)}) collective-permute-start(bf16[528,128]{1,0:T(8,128)(2,1)S(1)} %collective-permute-done.45.refs_3_), channel_id=1, source_target_pairs={{0,62},{1,63},{2,0},{3,1},{4,2},{5,3},{6,4},{7,5},{8,6},{9,7},{10,... | collective-permute-start | bytes 405512 | tf_op jit(solution)/shard_map/ppermute | solution.py:25
  192.5 31.7 %collective-permute-start.48 = (bf16[1024,128]{1,0:T(8,128)(2,1)}, bf16[1024,128]{1,0:T(8,128)(2,1)S(1)}, u32[]{:S(2)}, u32[]{:S(2)}) collective-permute-start(bf16[1024,128]{1,0:T(8,128)(2,1)} %collective-permute-done.44.refs_2_), channel_id=1, source_target_pairs={{0,2},{1,3},{2,4},{3,5},{4,6},{5,7},{6,8},{7,9},{8,10},{9,11},{10,... | collective-permute-start | bytes 786440 | tf_op jit(solution)/shard_map/ppermute | solution.py:25
  192.5 31.8 %collective-permute-start.50 = (bf16[1024,128]{1,0:T(8,128)(2,1)}, bf16[1024,128]{1,0:T(8,128)(2,1)S(1)}, u32[]{:S(2)}, u32[]{:S(2)}) collective-permute-start(bf16[1024,128]{1,0:T(8,128)(2,1)} %collective-permute-done.46.refs_4_), channel_id=1, source_target_pairs={{0,62},{1,63},{2,0},{3,1},{4,2},{5,3},{6,4},{7,5},{8,6},{9,7},{10,... | collective-permute-start | bytes 786440 | tf_op jit(solution)/shard_map/ppermute | solution.py:25
  206.4 14.3 %collective-permute-start.51 = (bf16[528,128]{1,0:T(8,128)(2,1)S(1)}, bf16[528,128]{1,0:T(8,128)(2,1)S(1)}, u32[]{:S(2)}, u32[]{:S(2)}) collective-permute-start(bf16[528,128]{1,0:T(8,128)(2,1)S(1)} %collective-permute-done.47.refs_5_), channel_id=1, source_target_pairs={{0,2},{1,3},{2,4},{3,5},{4,6},{5,7},{6,8},{7,9},{8,10},{9,11},{10,... | collective-permute-start | bytes 405512 | tf_op jit(solution)/shard_map/ppermute | solution.py:25
  220.8 17.6 %collective-permute-start.55 = (bf16[528,128]{1,0:T(8,128)(2,1)S(1)}, bf16[528,128]{1,0:T(8,128)(2,1)S(1)}, u32[]{:S(2)}, u32[]{:S(2)}) collective-permute-start(bf16[528,128]{1,0:T(8,128)(2,1)S(1)} %collective-permute-done.51.refs_1_), channel_id=1, source_target_pairs={{0,2},{1,3},{2,4},{3,5},{4,6},{5,7},{6,8},{7,9},{8,10},{9,11},{10,... | collective-permute-start | bytes 405512 | tf_op jit(solution)/shard_map/ppermute | solution.py:25
  220.9 17.6 %collective-permute-start.57 = (bf16[528,128]{1,0:T(8,128)(2,1)S(1)}, bf16[528,128]{1,0:T(8,128)(2,1)S(1)}, u32[]{:S(2)}, u32[]{:S(2)}) collective-permute-start(bf16[528,128]{1,0:T(8,128)(2,1)S(1)} %collective-permute-done.53.refs_3_), channel_id=1, source_target_pairs={{0,62},{1,63},{2,0},{3,1},{4,2},{5,3},{6,4},{7,5},{8,6},{9,7},{10,... | collective-permute-start | bytes 405512 | tf_op jit(solution)/shard_map/ppermute | solution.py:25
  224.1 17.6 %collective-permute-start.52 = (bf16[512,128]{1,0:T(8,128)(2,1)S(1)}, bf16[512,128]{1,0:T(8,128)(2,1)S(1)}, u32[]{:S(2)}, u32[]{:S(2)}) collective-permute-start(bf16[512,128]{1,0:T(8,128)(2,1)S(1)} %slice.18), channel_id=1, source_target_pairs={{0,2},{1,3},{2,4},{3,5},{4,6},{5,7},{6,8},{7,9},{8,10},{9,11},{10,... | collective-permute-start | bytes 393224 | tf_op jit(solution)/shard_map/ppermute | solution.py:25
  224.3 17.4 %collective-permute-start.54 = (bf16[512,128]{1,0:T(8,128)(2,1)S(1)}, bf16[512,128]{1,0:T(8,128)(2,1)S(1)}, u32[]{:S(2)}, u32[]{:S(2)}) collective-permute-start(bf16[512,128]{1,0:T(8,128)(2,1)S(1)} %slice.19), channel_id=1, source_target_pairs={{0,62},{1,63},{2,0},{3,1},{4,2},{5,3},{6,4},{7,5},{8,6},{9,7},{10,... | collective-permute-start | bytes 393224 | tf_op jit(solution)/shard_map/ppermute | solution.py:25
  238.4 17.0 %collective-permute-start.59 = (bf16[528,128]{1,0:T(8,128)(2,1)S(1)}, bf16[528,128]{1,0:T(8,128)(2,1)S(1)}, u32[]{:S(2)}, u32[]{:S(2)}) collective-permute-start(bf16[528,128]{1,0:T(8,128)(2,1)S(1)} %collective-permute-done.55.refs_5_), channel_id=1, source_target_pairs={{0,2},{1,3},{2,4},{3,5},{4,6},{5,7},{6,8},{7,9},{8,10},{9,11},{10,... | collective-permute-start | bytes 405512 | tf_op jit(solution)/shard_map/ppermute | solution.py:25
  238.6 17.0 %collective-permute-start.60 = (bf16[528,128]{1,0:T(8,128)(2,1)S(1)}, bf16[528,128]{1,0:T(8,128)(2,1)S(1)}, u32[]{:S(2)}, u32[]{:S(2)}) collective-permute-start(bf16[528,128]{1,0:T(8,128)(2,1)S(1)} %collective-permute-done.57.refs_7_), channel_id=1, source_target_pairs={{0,62},{1,63},{2,0},{3,1},{4,2},{5,3},{6,4},{7,5},{8,6},{9,7},{10,... | collective-permute-start | bytes 405512 | tf_op jit(solution)/shard_map/ppermute | solution.py:25
  241.8 17.0 %collective-permute-start.56 = (bf16[512,128]{1,0:T(8,128)(2,1)S(1)}, bf16[512,128]{1,0:T(8,128)(2,1)S(1)}, u32[]{:S(2)}, u32[]{:S(2)}) collective-permute-start(bf16[512,128]{1,0:T(8,128)(2,1)S(1)} %collective-permute-done.52.refs_2_), channel_id=1, source_target_pairs={{0,2},{1,3},{2,4},{3,5},{4,6},{5,7},{6,8},{7,9},{8,10},{9,11},{10,... | collective-permute-start | bytes 393224 | tf_op jit(solution)/shard_map/ppermute | solution.py:25
  241.8 17.0 %collective-permute-start.58 = (bf16[512,128]{1,0:T(8,128)(2,1)S(1)}, bf16[512,128]{1,0:T(8,128)(2,1)S(1)}, u32[]{:S(2)}, u32[]{:S(2)}) collective-permute-start(bf16[512,128]{1,0:T(8,128)(2,1)S(1)} %collective-permute-done.54.refs_4_), channel_id=1, source_target_pairs={{0,62},{1,63},{2,0},{3,1},{4,2},{5,3},{6,4},{7,5},{8,6},{9,7},{10,... | collective-permute-start | bytes 393224 | tf_op jit(solution)/shard_map/ppermute | solution.py:25
  255.4 16.4 %collective-permute-start.61 = (bf16[528,128]{1,0:T(8,128)(2,1)S(1)}, bf16[528,128]{1,0:T(8,128)(2,1)S(1)}, u32[]{:S(2)}, u32[]{:S(2)}) collective-permute-start(bf16[528,128]{1,0:T(8,128)(2,1)S(1)} %collective-permute-done.59.refs_1_), channel_id=1, source_target_pairs={{0,2},{1,3},{2,4},{3,5},{4,6},{5,7},{6,8},{7,9},{8,10},{9,11},{10,... | collective-permute-start | bytes 405512 | tf_op jit(solution)/shard_map/ppermute | solution.py:25
  255.6 16.3 %collective-permute-start.62 = (bf16[528,128]{1,0:T(8,128)(2,1)S(1)}, bf16[528,128]{1,0:T(8,128)(2,1)S(1)}, u32[]{:S(2)}, u32[]{:S(2)}) collective-permute-start(bf16[528,128]{1,0:T(8,128)(2,1)S(1)} %collective-permute-done.60.refs_2_), channel_id=1, source_target_pairs={{0,62},{1,63},{2,0},{3,1},{4,2},{5,3},{6,4},{7,5},{8,6},{9,7},{10,... | collective-permute-start | bytes 405512 | tf_op jit(solution)/shard_map/ppermute | solution.py:25
  269.7 14.6 %collective-permute-start.79 = (bf16[512,128]{1,0:T(8,128)(2,1)}, bf16[512,128]{1,0:T(8,128)(2,1)S(1)}, u32[]{:S(2)}, u32[]{:S(2)}) collective-permute-start(bf16[512,128]{1,0:T(8,128)(2,1)} %get-tuple-element.108), channel_id=1, source_target_pairs={{0,62},{1,63},{2,0},{3,1},{4,2},{5,3},{6,4},{7,5},{8,6},{9,7},{10,... | collective-permute-start | bytes 393224 | tf_op jit(solution)/shard_map/ppermute | solution.py:25
  269.9 17.2 %collective-permute-start.109 = (bf16[512,128]{1,0:T(8,128)(2,1)}, bf16[512,128]{1,0:T(8,128)(2,1)S(1)}, u32[]{:S(2)}, u32[]{:S(2)}) collective-permute-start(bf16[512,128]{1,0:T(8,128)(2,1)} %get-tuple-element.138), channel_id=1, source_target_pairs={{0,2},{1,3},{2,4},{3,5},{4,6},{5,7},{6,8},{7,9},{8,10},{9,11},{10,... | collective-permute-start | bytes 393224 | tf_op jit(solution)/shard_map/ppermute | solution.py:25
  293.4 15.7 %collective-permute-start.81 = (bf16[1024,128]{1,0:T(8,128)(2,1)S(1)}, bf16[1024,128]{1,0:T(8,128)(2,1)S(1)}, u32[]{:S(2)}, u32[]{:S(2)}) collective-permute-start(bf16[1024,128]{1,0:T(8,128)(2,1)S(1)} %add_convert_fusion.33), channel_id=1, source_target_pairs={{0,62},{1,63},{2,0},{3,1},{4,2},{5,3},{6,4},{7,5},{8,6},{9,7},{10,... | collective-permute-start | bytes 786440 | tf_op jit(solution)/shard_map/ppermute | solution.py:25
  296.8 15.8 %collective-permute-start.111 = (bf16[1024,128]{1,0:T(8,128)(2,1)S(1)}, bf16[1024,128]{1,0:T(8,128)(2,1)S(1)}, u32[]{:S(2)}, u32[]{:S(2)}) collective-permute-start(bf16[1024,128]{1,0:T(8,128)(2,1)S(1)} %add_convert_fusion.11), channel_id=1, source_target_pairs={{0,2},{1,3},{2,4},{3,5},{4,6},{5,7},{6,8},{7,9},{8,10},{9,11},{10,... | collective-permute-start | bytes 786440 | tf_op jit(solution)/shard_map/ppermute | solution.py:25
  309.2 16.9 %collective-permute-start.82 = (bf16[1024,128]{1,0:T(8,128)(2,1)S(1)}, bf16[1024,128]{1,0:T(8,128)(2,1)S(1)}, u32[]{:S(2)}, u32[]{:S(2)}) collective-permute-start(bf16[1024,128]{1,0:T(8,128)(2,1)S(1)} %add_convert_fusion.32), channel_id=1, source_target_pairs={{0,62},{1,63},{2,0},{3,1},{4,2},{5,3},{6,4},{7,5},{8,6},{9,7},{10,... | collective-permute-start | bytes 786440 | tf_op jit(solution)/shard_map/ppermute | solution.py:25
  312.6 16.9 %collective-permute-start.112 = (bf16[1024,128]{1,0:T(8,128)(2,1)S(1)}, bf16[1024,128]{1,0:T(8,128)(2,1)S(1)}, u32[]{:S(2)}, u32[]{:S(2)}) collective-permute-start(bf16[1024,128]{1,0:T(8,128)(2,1)S(1)} %add_convert_fusion.10), channel_id=1, source_target_pairs={{0,2},{1,3},{2,4},{3,5},{4,6},{5,7},{6,8},{7,9},{8,10},{9,11},{10,... | collective-permute-start | bytes 786440 | tf_op jit(solution)/shard_map/ppermute | solution.py:25
  (206 other events, 3460.8 us)
